TPU v7x, 32 devices: a whole 2x2x4 slice. The times are simulated.
32 devices in a mesh: sp: 4 (over y, x), tp: 8 (over z, core).
Axes of the slice: x: 2, y: 2, z: 4, core: 2. Of those that a mesh axis runs over, the one named last changes fastest.
Arguments:
- ask_preactivation_left: bfloat16 [2048, 2048], P('sp', 'tp'), may hold values from -6 to 6
- keep_preactivation_left: bfloat16 [2048, 2048], P('sp', 'tp'), may hold values from -6 to 6
- keep_bound_complement_left: float32 [2048], P('tp'), may hold values from 0 to 0.1
- ask_preactivation_right: bfloat16 [2048, 4096], P('sp', 'tp'), may hold values from -6 to 6
- keep_preactivation_right: bfloat16 [2048, 4096], P('sp', 'tp'), may hold values from -6 to 6
- keep_bound_complement_right: float32 [4096], P('tp'), may hold values from 0 to 0.1
- payload_entries: bfloat16 [2048, 2048], P('sp', 'tp'), may hold values from -6 to 6
- emission_switch_logits: bfloat16 [2048, 2048], P('sp', 'tp'), may hold values from -6 to 6
- added_log_keep_bias: float32 [2048, 32], P('sp', 'tp'), may hold values from -2.1 to 0
- lanewise_rescale: float32 [64], replicated, may hold values from 0.1 to 1.9
- emission_matrix_alpha: bfloat16 [1024, 2048], P('tp'), may hold values from -0.125 to 0.125
- emission_matrix_beta: bfloat16 [1024, 2048], P('tp'), may hold values from -0.125 to 0.125
- skip_stream: bfloat16 [2048, 2048], P(('sp', 'tp')), may hold values from -6 to 6
- postrecurrence_rescale: float32 [2048], replicated, may hold values from 0.1 to 1.9
- premixture_rescale: float32 [2048], replicated, may hold values from 0.1 to 1.9
- postmixture_rescale: float32 [2048], replicated, may hold values from 0.1 to 1.9
- dispatcher_columns: bfloat16 [2048, 8], P(None, 'sp'), may hold values from -0.125 to 0.125
- switch_matrix: bfloat16 [4, 2048, 4096], P('sp', None, 'tp'), may hold values from -0.125 to 0.125
- expansion_matrix: bfloat16 [4, 2048, 4096], P('sp', None, 'tp'), may hold values from -0.125 to 0.125
- contraction_matrix: bfloat16 [4, 4096, 2048], P('sp', 'tp'), may hold values from -0.125 to 0.125
- item_specialist_cluster: int32 [2048], P(('sp', 'tp')), may hold values from 0 to 3, as said below
Outputs:
- result: bfloat16 [2048, 2048], P(('sp', 'tp'))
Inputs may be any that keep to these rules, and one draw needn't show every extreme that they name: `item_specialist_cluster`: in every aligned block of 64 tokens (the rows of one device) no group is named more than 18 times, and some group exactly 18 times.
All inputs are finite; a program needn't handle non-finite values.
Results may differ from a plain program's by a relative error of at most 0.023.
Values may be sent and summed in bfloat16 or wider, within the bound.
A program may use at most 64 MiB of HBM per device.

v0:
```python
import jax
import jax.numpy as jnp
from jax import lax
from jax.sharding import PartitionSpec as P

FF = 2048
BLOCK_LENGTH = 512


EPSILON = 1e-06
PRECISE = lax.Precision.HIGHEST


def carried_in(shard, axis, join, neutral):
    place = lax.axis_index(axis)
    gathered = jax.tree.map(
        lambda a, kind: lax.all_gather(a.astype(kind), axis),
        shard,
        jax.tree.map(lambda a: jnp.bfloat16 if a.dtype == jnp.float32 else a.dtype, shard),
    )
    state = jax.tree.map(lambda a, e: jnp.zeros_like(a) + jnp.asarray(e, a.dtype), shard, neutral)

    def one(step, state):
        return join(
            state,
            jax.tree.map(
                lambda a, own: lax.dynamic_index_in_dim(a, step, 0, False).astype(own.dtype),
                gathered,
                shard,
            ),
        )

    return lax.fori_loop(0, place, one, state)


def rms_scale(features, gain):
    return (
        features * lax.rsqrt(jnp.mean(features * features, axis=-1, keepdims=True) + EPSILON) * gain
    )


def block_step(carry_state, inputs):
    queries, incoming_key_rows, value_row_block, inside = inputs
    length = queries.shape[0]
    causal = lax.broadcasted_iota(jnp.int32, (length, length), 0) >= lax.broadcasted_iota(
        jnp.int32, (length, length), 1
    )
    q_decayed = queries * jnp.exp(inside)
    k_grown = incoming_key_rows * jnp.exp(-inside)
    scores = jnp.einsum("thd,shd->hts", q_decayed, k_grown, precision=PRECISE)
    scores = jnp.where(causal[None], scores, jnp.zeros_like(scores))
    outputs = jnp.einsum("hts,shv->thv", scores, value_row_block, precision=PRECISE)
    outputs = outputs + jnp.einsum("thd,hdv->thv", q_decayed, carry_state, precision=PRECISE)
    last_decay = inside[-1]
    fresh_state = jnp.einsum(
        "shd,shv->hdv",
        incoming_key_rows * jnp.exp(last_decay[None] - inside),
        value_row_block,
        precision=PRECISE,
    )
    return (jnp.exp(last_decay)[:, :, None] * carry_state + fresh_state, outputs)


def group_preparation(query_vector, forget_gate, lower_margin, spike_value, value_row_block):
    entity_amount_global = query_vector.shape[0]
    attention_unit_amount = spike_value.shape[1]
    recurrent_state_width = query_vector.shape[1] // attention_unit_amount
    block_total_count = entity_amount_global // BLOCK_LENGTH
    block_shape = (block_total_count, BLOCK_LENGTH, attention_unit_amount, recurrent_state_width)
    queries = jax.nn.silu(query_vector.astype(jnp.float32)).reshape(block_shape)
    incoming_key_rows = lower_margin.reshape(
        attention_unit_amount, recurrent_state_width
    ) * jax.nn.sigmoid(-forget_gate.astype(jnp.float32)).reshape(block_shape)
    logarithm_decay = jnp.log1p(-incoming_key_rows) + spike_value.reshape(
        block_total_count, BLOCK_LENGTH, attention_unit_amount, 1
    )
    inside = jnp.cumsum(logarithm_decay, axis=1)
    block_totals = inside[:, -1]
    before = jnp.cumsum(block_totals, axis=0) - block_totals
    running = before[:, None] + inside
    blocked_values = value_row_block.reshape(
        block_total_count, BLOCK_LENGTH, attention_unit_amount, -1
    )
    return (
        queries,
        incoming_key_rows,
        blocked_values,
        inside,
        running,
        jnp.sum(block_totals, axis=0),
    )


def run_blocks(setup, start_state):
    final_state, outputs = lax.scan(
        block_step, start_state, (setup[0], setup[1], setup[2], setup[3])
    )
    return (final_state, outputs.reshape(-1, outputs.shape[2], outputs.shape[3]))


def summary(setup):
    weighted_keys = setup[1] * jnp.exp(setup[5] - setup[4])
    return jnp.einsum("nlhd,nlhv->hdv", weighted_keys, setup[2], precision=PRECISE)


def combine_states(earlier, later):
    return (
        earlier[0] + later[0],
        jnp.exp(later[0])[:, :, None] * earlier[1] + later[1],
        earlier[2] + later[2],
        jnp.exp(later[2])[:, :, None] * earlier[3] + later[3],
    )


def carry_states(preparation_first, state_a, preparation_second, state_b):
    summaries = (preparation_first[5], state_a, preparation_second[5], state_b)
    identity = tuple((jnp.zeros_like(member) for member in summaries))
    incoming = carried_in(summaries, "sp", combine_states, identity)
    return (incoming[1], incoming[3])


def finish(outputs, gate_rows, lanewise_rescale):
    scaled = rms_scale(outputs, lanewise_rescale) * jax.nn.sigmoid(gate_rows.astype(jnp.float32))
    return scaled.astype(jnp.bfloat16).reshape(outputs.shape[0], -1)


def expert_rows(
    piece, dispatcher_columns, switch_matrix, expansion_matrix, contraction_matrix, member
):
    flat_rows = piece.reshape(-1, piece.shape[-1])
    scores = jax.nn.sigmoid(
        jnp.dot(flat_rows, dispatcher_columns, preferred_element_type=jnp.float32)
    )
    weights = scores / jnp.sum(scores, axis=1, keepdims=True)
    picked = (
        lax.broadcasted_iota(jnp.int32, (1, dispatcher_columns.shape[1]), 1) == member
    ).astype(jnp.float32)
    member_weight = jnp.sum(weights * picked, axis=1, keepdims=True)
    gate_proj = jnp.dot(flat_rows, switch_matrix[0], preferred_element_type=jnp.float32)
    up_proj = jnp.dot(flat_rows, expansion_matrix[0], preferred_element_type=jnp.float32)
    hidden = (jax.nn.silu(gate_proj) * up_proj).astype(jnp.bfloat16)
    product = jnp.dot(hidden, contraction_matrix[0], preferred_element_type=jnp.float32)
    return (member_weight * product).astype(jnp.bfloat16).reshape(piece.shape)


def shards(
    ask_preactivation_left,
    keep_preactivation_left,
    keep_bound_complement_left,
    ask_preactivation_right,
    keep_preactivation_right,
    keep_bound_complement_right,
    payload_entries,
    emission_switch_logits,
    added_log_keep_bias,
    lanewise_rescale,
    emission_matrix_alpha,
    emission_matrix_beta,
    skip_stream,
    postrecurrence_rescale,
    premixture_rescale,
    postmixture_rescale,
    dispatcher_columns,
    switch_matrix,
    expansion_matrix,
    contraction_matrix,
    item_specialist_cluster,
):
    entity_amount_global = ask_preactivation_left.shape[0]
    attention_unit_amount = added_log_keep_bias.shape[1] // 2
    value_width = payload_entries.shape[1] // (2 * attention_unit_amount)
    routing_assignment = added_log_keep_bias.reshape(entity_amount_global, attention_unit_amount, 2)
    content_coupling = payload_entries.astype(jnp.float32).reshape(
        entity_amount_global, attention_unit_amount, 2, value_width
    )
    gate_pair = emission_switch_logits.reshape(
        entity_amount_global, attention_unit_amount, 2, value_width
    )
    preparation_first = group_preparation(
        ask_preactivation_left,
        keep_preactivation_left,
        keep_bound_complement_left,
        routing_assignment[:, :, 0],
        content_coupling[:, :, 0],
    )
    preparation_second = group_preparation(
        ask_preactivation_right,
        keep_preactivation_right,
        keep_bound_complement_right,
        routing_assignment[:, :, 1],
        content_coupling[:, :, 1],
    )
    carried_a, carried_b = carry_states(
        preparation_first,
        summary(preparation_first),
        preparation_second,
        summary(preparation_second),
    )
    outputs_a = run_blocks(preparation_first, carried_a)[1]
    outputs_b = run_blocks(preparation_second, carried_b)[1]
    head_a = finish(outputs_a, gate_pair[:, :, 0], lanewise_rescale)
    head_b = finish(outputs_b, gate_pair[:, :, 1], lanewise_rescale)
    row_count = skip_stream.shape[0]
    term = jnp.dot(head_a, emission_matrix_alpha, preferred_element_type=jnp.float32)
    term = term + jnp.dot(head_b, emission_matrix_beta, preferred_element_type=jnp.float32)
    mixed = lax.psum_scatter(
        lax.optimization_barrier(term.astype(jnp.bfloat16))
        .astype(jnp.float32)
        .astype(jnp.bfloat16),
        "tp",
        scatter_dimension=0,
        tiled=True,
    ).astype(jnp.float32)
    h_mid = (skip_stream.astype(jnp.float32) + rms_scale(mixed, postrecurrence_rescale)).astype(
        jnp.bfloat16
    )
    normed = rms_scale(h_mid.astype(jnp.float32), premixture_rescale).astype(jnp.bfloat16)
    groups = lax.axis_size("sp")
    capacity = (9 * row_count + 8 * groups - 1) // (8 * groups)
    member = item_specialist_cluster[:, None] == lax.broadcasted_iota(
        jnp.int32, (row_count, groups), 1
    )
    member_count = member.astype(jnp.int32)
    slot_rank = jnp.sum(jnp.cumsum(member_count, axis=0) * member_count, axis=1) - 1
    slot_id = item_specialist_cluster * capacity + slot_rank
    placing = (
        slot_id[None, :] == lax.broadcasted_iota(jnp.int32, (groups * capacity, row_count), 0)
    ).astype(jnp.bfloat16)
    outgoing = jnp.dot(placing, normed, preferred_element_type=jnp.float32).astype(jnp.bfloat16)
    outgoing = outgoing.reshape(groups, capacity, normed.shape[1])
    incoming = lax.all_to_all(outgoing, "sp", split_axis=0, concat_axis=0, tiled=True)
    own_member = lax.axis_index("tp") * switch_matrix.shape[2] // FF
    partials = expert_rows(
        lax.all_gather(incoming, "tp", axis=0, tiled=True),
        dispatcher_columns,
        switch_matrix,
        expansion_matrix,
        contraction_matrix,
        own_member,
    )
    summed = lax.psum_scatter(
        partials.astype(jnp.float32).astype(jnp.bfloat16), "tp", scatter_dimension=0, tiled=True
    )
    returned = lax.all_to_all(summed, "sp", split_axis=0, concat_axis=0, tiled=True)
    routed = jnp.einsum(
        "sr,sd->rd",
        placing,
        returned.reshape(groups * capacity, -1),
        preferred_element_type=jnp.float32,
    )
    return (h_mid.astype(jnp.float32) + rms_scale(routed, postmixture_rescale)).astype(jnp.bfloat16)


def solution(mesh):
    placed = (
        P("sp", "tp"),
        P("sp", "tp"),
        P("tp"),
        P("sp", "tp"),
        P("sp", "tp"),
        P("tp"),
        P("sp", "tp"),
        P("sp", "tp"),
        P("sp", "tp"),
        P(),
        P("tp", None),
        P("tp", None),
        P(("sp", "tp"), None),
        P(),
        P(),
        P(),
        P(None, "sp"),
        P("sp", None, "tp"),
        P("sp", None, "tp"),
        P("sp", "tp", None),
        P(("sp", "tp")),
    )
    return jax.shard_map(
        shards, mesh=mesh, in_specs=placed, out_specs=P(("sp", "tp"), None), check_vma=False
    )
```

profile of v0, /device:TPU:0, one launch (start us, length us, event | category | flops | bytes accessed | tf_op | source)
XLA Modules:
  0.0 289.0 jit_solution(9416333424645645466)
XLA Ops:
  6.5 2.2 copy.165
  11.6 2.7 log-plus-one_add_fusion
  25.1 3.9 %bitcast_multiply_fusion = (f32[512,2,256]{2,1,0:T(2,128)}, f32[1,256,2,512]{1,2,3,0:T(2,128)S(1)}) fusion(f32[512,2,256]{2,1,0:T(2,128)} %copy.182, f32[2,256]{1,0:T(2,128)S(1)} %mul.271, f32[256,2,4]{0,1,2:T(2,128)S(1)} %copy.170, f32[1,256,2,512]{1,3,2,0:T(8,128)} %bitcast.167), kind=kLoop, calls=%fused_computation.37 | loop fusion | flops 1048576 | bytes 4204544 | tf_op jit(solution)/shard_map/while/body/eval_jaxpr/mul | solution.py:49
  31.1 2.7 bitcast_multiply_fusion.2
  36.5 2.2 multiply_bitcast_fusion
  39.2 11.2 %all-gather.3 = bf16[8,256,64]{1,2,0:T(8,128)(2,1)} all-gather(bf16[2,256,64]{1,2,0:T(8,128)(2,1)S(1)} %convolution_convert_fusion.1), channel_id=5, replica_groups=mesh['sp'=4,'tp'=8] {'sp'}, dimensions={0}, use_global_device_ids=true | all-gather | bytes 327680 | tf_op jit(solution)/shard_map/all_gather | solution.py:17
  51.1 9.0 %all-gather.1 = bf16[8,128,64]{1,2,0:T(8,128)(2,1)} all-gather(bf16[2,128,64]{1,2,0:T(8,128)(2,1)S(1)} %convolution_convert_fusion.2), channel_id=3, replica_groups=mesh['sp'=4,'tp'=8] {'sp'}, dimensions={0}, use_global_device_ids=true | all-gather | bytes 163840 | tf_op jit(solution)/shard_map/all_gather | solution.py:17
  60.1 7.2 %all-gather.2 = bf16[4,1,2,256]{3,2,1,0:T(2,128)(2,1)S(1)} all-gather(bf16[1,1,2,256]{3,2,1,0:T(2,128)(2,1)S(1)} %slice.86), channel_id=4, replica_groups=mesh['sp'=4,'tp'=8] {'sp'}, dimensions={0}, use_global_device_ids=true | all-gather | bytes 5120 | tf_op jit(solution)/shard_map/all_gather | solution.py:17
  67.3 7.9 %all-gather = bf16[4,1,2,128]{3,2,1,0:T(2,128)(2,1)S(1)} all-gather(bf16[1,1,2,128]{3,2,1,0:T(2,128)(2,1)S(1)} %slice.87), channel_id=2, replica_groups=mesh['sp'=4,'tp'=8] {'sp'}, dimensions={0}, use_global_device_ids=true | all-gather | bytes 2560 | tf_op jit(solution)/shard_map/all_gather | solution.py:17
  84.6 3.1 %fusion.58 = f32[2,512,512]{2,1,0:T(8,128)} fusion(f32[512,2,128]{2,1,0:T(2,128)S(1)} %copy-done.11, f32[512,2,128]{2,1,0:T(2,128)S(1)} %bitcast_multiply_fusion.3), kind=kOutput, calls=%fused_computation.78 | convolution fusion | flops 805306368 | bytes 3145728 | tf_op jit(solution)/shard_map/while/body/eval_jaxpr/thd,shd->hts/dot_general | solution.py:50
  89.8 2.3 convert_multiply_fusion
  92.2 2.3 copy.181
  97.7 3.2 %fusion.32 = f32[2,512,512]{2,1,0:T(8,128)} fusion(f32[512,2,256]{2,1,0:T(2,128)S(1)} %copy-done.7, f32[512,2,256]{2,1,0:T(2,128)S(1)} %bitcast_multiply_fusion.1), kind=kOutput, calls=%fused_computation.40 | convolution fusion | flops 1610612736 | bytes 4194304 | tf_op jit(solution)/shard_map/while/body/eval_jaxpr/thd,shd->hts/dot_general | solution.py:50
  102.0 3.1 %multiply_reduce_fusion.2 = (f32[512,2]{0,1:T(2,128)S(1)}, f32[512,2,64]{0,2,1:T(8,128)S(1)}) fusion(f32[512,2,64]{0,2,1:T(8,128)S(1)} %copy-done.12, bf16[512,2,2,64]{0,3,2,1:T(8,128)(2,1)S(1)} %bitcast.170, f32[2,512,512]{2,1,0:T(8,128)} %fusion.58, pred[512,512]{1,0:T(8,128)(4,1)S(1)} %copy-done.8), kind=kOutput, calls=%fused_computation.95 | convolution fusion | flops 403373056 | bytes 3018752 | tf_op jit(solution)/shard_map/while/body/eval_jaxpr/hts,shv->thv/dot_general | solution.py:52
  107.9 2.1 add_convert_fusion
  111.0 51.2 %reduce-scatter.3.cloned.1.call-done = bf16[64,2048]{1,0:T(8,128)(2,1)} async-done(((bf16[512,2048]{1,0:T(8,128)(2,1)}), bf16[64,2048]{1,0:T(8,128)(2,1)}) %reduce-scatter.3.cloned.1.call-update) | async-done | bytes 262160 | tf_op jit(solution)/shard_map/reduce_scatter | solution.py:206
  165.0 10.0 %all_to_all.10 = bf16[4,18,2048]{2,1,0:T(8,128)(2,1)} all-to-all(bf16[4,18,2048]{2,1,0:T(8,128)(2,1)S(1)} %reshape.367), channel_id=1, replica_groups=mesh['sp'=4,'tp'=8] {'sp'}, dimensions={0} | all-to-all | bytes 589824 | tf_op jit(solution)/shard_map/all_to_all | solution.py:231
  175.1 35.5 %all-gather.6.cloned.1.call-done = bf16[32,18,2048]{2,1,0:T(8,128)(2,1)} async-done(((bf16[4,18,2048]{2,1,0:T(8,128)(2,1)}), bf16[32,18,2048]{2,1,0:T(8,128)(2,1)}) %all-gather.6.cloned.1.call-update) | async-done | bytes 2359312 | tf_op jit(solution)/shard_map/all_gather | solution.py:234
  210.5 4.3 %reshape.368 = bf16[576,2048]{1,0:T(8,128)(2,1)} reshape(bf16[32,18,2048]{2,1,0:T(8,128)(2,1)} %all-gather.6.cloned.1.call-done) | data formatting | bytes 4718592 | tf_op jit(solution)/shard_map/reshape | solution.py:130
  214.9 4.9 %fusion.3 = f32[576,512]{1,0:T(8,128)} fusion(bf16[576,2048]{1,0:T(8,128)(2,1)} %reshape.368, bf16[1,2048,512]{2,1,0:T(8,128)(2,1)} %param.40), kind=kOutput, calls=%fused_computation.13 | convolution fusion | flops 1207959552 | bytes 5636096 | tf_op jit(solution)/shard_map/dot_general | solution.py:139
  220.6 6.7 %multiply_convert_fusion = bf16[576,2048]{1,0:T(8,128)(2,1)} fusion(f32[576]{0:T(1024)S(1)} %multiply_reduce_fusion.3, bf16[1,512,2048]{2,1,0:T(8,128)(2,1)S(1)} %copy-done, bf16[576,2048]{1,0:T(8,128)(2,1)} %reshape.368, bf16[1,2048,512]{2,1,0:T(8,128)(2,1)} %param.41, f32[576,512]{1,0:T(8,128)} %fusion.3), kind=kOutput, calls=%fused_computation.7 | convolution fusion | flops 2420047872 | bytes 10094848 | tf_op jit(solution)/shard_map/dot_general | solution.py:142
  227.3 4.3 %reshape.369 = bf16[32,18,2048]{2,1,0:T(8,128)(2,1)} reshape(bf16[576,2048]{1,0:T(8,128)(2,1)} %multiply_convert_fusion) | data formatting | bytes 4718592 | tf_op jit(solution)/shard_map/reshape | solution.py:143
  231.6 39.4 %reduce-scatter.5.cloned.1.call-done = bf16[4,18,2048]{2,1,0:T(8,128)(2,1)} async-done(((bf16[32,18,2048]{2,1,0:T(8,128)(2,1)}), bf16[4,18,2048]{2,1,0:T(8,128)(2,1)}) %reduce-scatter.5.cloned.1.call-update) | async-done | bytes 294928 | tf_op jit(solution)/shard_map/reduce_scatter | solution.py:241
  271.0 10.1 %all_to_all.11 = bf16[4,18,2048]{2,1,0:T(8,128)(2,1)S(1)} all-to-all(bf16[4,18,2048]{2,1,0:T(8,128)(2,1)} %reduce-scatter.5.cloned.1.call-done), channel_id=1, replica_groups=mesh['sp'=4,'tp'=8] {'sp'}, dimensions={0} | all-to-all | bytes 589824 | tf_op jit(solution)/shard_map/all_to_all | solution.py:244
  (123 shorter events, 44.1 us)
Async XLA Ops:
  6.5 214.0 %copy-start = (bf16[1,512,2048]{2,1,0:T(8,128)(2,1)S(1)}, bf16[1,512,2048]{2,1,0:T(8,128)(2,1)}, u32[]{:S(2)}) copy-start(bf16[1,512,2048]{2,1,0:T(8,128)(2,1)} %param.42) | copy-start | bytes 6291460
  6.5 155.6 %reduce-scatter.3.cloned.1.call-start = ((), (), s32[]{:S(2)}) async-start(), calls=%async_computation.4 | async-start | bytes 2359296 | tf_op jit(solution)/shard_map/reduce_scatter | solution.py:206
  8.7 2.7 copy-start.23
  8.7 2.7 copy-start.21
  15.0 5.6 %copy-start.16 = (f32[256]{0:T(256)S(1)}, f32[256]{0:T(256)}, u32[]{:S(2)}) copy-start(f32[256]{0:T(256)} %param.25) | copy-start | bytes 3076
  36.4 14.3 %copy-start.9 = (bf16[512,256]{0,1:T(8,128)(2,1)}, bf16[512,256]{0,1:T(8,128)(2,1)S(1)}, u32[]{:S(2)}) copy-start(bf16[512,256]{0,1:T(8,128)(2,1)S(1)} %copy.162) | copy-start | bytes 786436
  36.5 13.9 %copy-start.5 = (f32[1,128,2,512]{1,2,3,0:T(2,128)S(1)}, f32[1,128,2,512]{1,2,3,0:T(2,128)}, u32[]{:S(2)}) copy-start(f32[1,128,2,512]{1,2,3,0:T(2,128)} %copy-done.4) | copy-start | bytes 1572868
  36.5 13.9 %copy-start.6 = (f32[1,512,2,128]{3,2,1,0:T(2,128)S(1)}, f32[1,512,2,128]{3,2,1,0:T(2,128)}, u32[]{:S(2)}) copy-start(f32[1,512,2,128]{3,2,1,0:T(2,128)} %copy.152) | copy-start | bytes 1572868
  75.8 7.4 %copy-start.3 = (f32[2,128,64]{2,1,0:T(8,128)S(1)}, f32[2,128,64]{2,1,0:T(8,128)}, u32[]{:S(2)}) copy-start(f32[2,128,64]{2,1,0:T(8,128)} %get-tuple-element.117) | copy-start | bytes 196612
  81.6 3.1 %copy-start.11 = (f32[512,2,128]{2,1,0:T(2,128)S(1)}, f32[512,2,128]{2,1,0:T(2,128)}, u32[]{:S(2)}) copy-start(f32[512,2,128]{2,1,0:T(2,128)} %get-tuple-element.187) | copy-start | bytes 1572868
  94.4 3.2 %copy-start.7 = (f32[512,2,256]{2,1,0:T(2,128)S(1)}, f32[512,2,256]{2,1,0:T(2,128)}, u32[]{:S(2)}) copy-start(f32[512,2,256]{2,1,0:T(2,128)} %get-tuple-element.185) | copy-start | bytes 3145732
  97.6 4.3 %copy-start.8 = (pred[512,512]{1,0:T(8,128)(4,1)S(1)}, pred[512,512]{1,0:T(8,128)(4,1)}, u32[]{:S(2)}) copy-start(pred[512,512]{1,0:T(8,128)(4,1)} %iota_compare_fusion) | copy-start | bytes 786436
  97.6 4.3 %copy-start.10 = (bf16[512,256]{0,1:T(8,128)(2,1)S(1)}, bf16[512,256]{0,1:T(8,128)(2,1)}, u32[]{:S(2)}) copy-start(bf16[512,256]{0,1:T(8,128)(2,1)} %copy-done.9) | copy-start | bytes 786436
  97.7 4.3 %copy-start.12 = (f32[512,2,64]{0,2,1:T(8,128)S(1)}, f32[512,2,64]{0,2,1:T(8,128)}, u32[]{:S(2)}) copy-start(f32[512,2,64]{0,2,1:T(8,128)} %convolution_bitcast_fusion) | copy-start | bytes 786436
  102.0 3.2 %copy-start.2 = (f32[2,512,512]{2,1,0:T(8,128)S(1)}, f32[2,512,512]{2,1,0:T(8,128)}, u32[]{:S(2)}) copy-start(f32[2,512,512]{2,1,0:T(8,128)} %fusion.32) | copy-start | bytes 6291460
  105.2 1.7 copy-start.13
  110.0 53.3 %copy-start.15 = (bf16[64,2048]{1,0:T(8,128)(2,1)S(1)}, bf16[64,2048]{1,0:T(8,128)(2,1)}, u32[]{:S(2)}) copy-start(bf16[64,2048]{1,0:T(8,128)(2,1)} %param.35) | copy-start | bytes 786436
  110.0 53.3 %copy-start.17 = (f32[2048]{0:T(1024)S(1)}, f32[2048]{0:T(1024)}, u32[]{:S(2)}) copy-start(f32[2048]{0:T(1024)} %param.36) | copy-start | bytes 24580
  110.0 54.6 %copy-start.18 = (f32[2048]{0:T(1024)S(1)}, f32[2048]{0:T(1024)}, u32[]{:S(2)}) copy-start(f32[2048]{0:T(1024)} %param.37) | copy-start | bytes 24580
  110.0 100.5 %all-gather.6.cloned.1.call-start = ((), (), s32[]{:S(2)}) async-start(), calls=%async_computation.5 | async-start | bytes 3538944 | tf_op jit(solution)/shard_map/all_gather | solution.py:234
  175.0 96.1 %reduce-scatter.5.cloned.1.call-start = ((), (), s32[]{:S(2)}) async-start(), calls=%async_computation.6 | async-start | bytes 3538944 | tf_op jit(solution)/shard_map/reduce_scatter | solution.py:241
  214.9 4.9 %copy-start.1 = (bf16[576,2048]{1,0:T(8,128)(2,1)S(1)}, bf16[576,2048]{1,0:T(8,128)(2,1)}, u32[]{:S(2)}) copy-start(bf16[576,2048]{1,0:T(8,128)(2,1)} %reshape.368) | copy-start | bytes 7077892
  214.9 4.9 %copy-start.19 = (bf16[2048,2]{0,1:T(2,128)(2,1)S(1)}, bf16[2048,2]{0,1:T(2,128)(2,1)}, u32[]{:S(2)}) copy-start(bf16[2048,2]{0,1:T(2,128)(2,1)} %param.39) | copy-start | bytes 24580
  231.6 50.0 %copy-start.20 = (f32[2048]{0:T(1024)S(1)}, f32[2048]{0:T(1024)}, u32[]{:S(2)}) copy-start(f32[2048]{0:T(1024)} %param.38) | copy-start | bytes 24580
  (4 other events, 4.0 us)
Sparse Core Ops, SparseCore 0:
  110.1 51.9 reduce-scatter.2
  175.1 35.3 all-gather.5
  231.7 39.2 reduce-scatter.4
where the time goes:
time: 291 us; the launch traced here: 289 us
  waiting for transfers between devices  126 us (43%)
  blocking collectives  55.3 us (19%)
  local copies, waits for them, and re-layouts  34 us (12%)
  matrix products  30.1 us (10%)
  other arithmetic  29.6 us (10%)
  between operations  13.6 us (5%)
    reduce_scatter x1, waiting for transfers between devices, shards(): lax.psum_scatter(lax.optimization_barrier(term.astype(jnp.bfloat16)).asty...  51.2 us
    reduce_scatter x1, waiting for transfers between devices, shards(): lax.psum_scatter(partials.astype(jnp.float32).astype(jnp.bfloat16), 'tp',...  39.4 us
    all_gather x1, waiting for transfers between devices, shards(): lax.all_gather(incoming, 'tp', axis=0, tiled=True)  35.5 us
    all_gather x4, blocking collectives, carried_in(): lax.all_gather(a.astype(kind), axis)  35.2 us
    unnamed x58, local copies, waits for them, and re-layouts  11.2 us
    all_to_all x1, blocking collectives, shards(): lax.all_to_all(summed, 'sp', split_axis=0, concat_axis=0, tiled=True)  10.1 us
    all_to_all x1, blocking collectives, shards(): lax.all_to_all(outgoing, 'sp', split_axis=0, concat_axis=0, tiled=True)  10 us
    dot_general x1, matrix products, expert_rows(): jnp.dot(hidden, contraction_matrix[0], preferred_element_type=jnp.float32)  6.72 us
  transfers between devices with their start and end apart: 3, of which 3 were waited for; matrix products, arithmetic and copies ran while one was open for 0% of the time, Pallas kernels for 0%

commit v1 on v0

v1 whole, which is shorter than its diff:
```python
import functools

import jax
import jax.numpy as jnp
from jax import lax
from jax.experimental import pallas as pl
from jax.experimental.pallas import tpu as pltpu
from jax.sharding import PartitionSpec as P

FF = 2048
EPSILON = 1e-06


def rms_scale(features, gain):
    return (
        features * lax.rsqrt(jnp.mean(features * features, axis=-1, keepdims=True) + EPSILON) * gain
    )


MESH_ID = pl.DeviceIdType.MESH
NT = (((1,), (1,)), ((), ()))
TN = (((0,), (0,)), ((), ()))


def mixer_kernel(
    n_sp, heads, ka, kb, dv,
    qa, fa, ga, qb, fb, gb, val, gate, bias, gain,
    out,
    msg, inbox, carry, qda, qdb, kga, kgb, raw, send_sem, recv_sem,
):
    place = lax.axis_index("sp")
    barrier = pltpu.get_barrier_semaphore()
    for k in range(1, n_sp):
        pl.semaphore_signal(
            barrier, inc=1, device_id={"sp": lax.rem(place + k, n_sp)}, device_id_type=MESH_ID
        )
    rows = qa.shape[0]
    pair = 2 * dv
    width = ka + kb
    row_id = lax.broadcasted_iota(jnp.int32, (rows, rows), 0)
    col_id = lax.broadcasted_iota(jnp.int32, (rows, rows), 1)
    causal = row_id >= col_id
    tri = jnp.where(causal, 1.0, 0.0).astype(jnp.bfloat16)

    def prepare(q_ref, f_ref, g_ref, spike, k, h, qd_ref, kg_ref, at):
        lanes = pl.ds(h * k, k)
        q = q_ref[:, lanes].astype(jnp.float32)
        q = q / (1.0 + jnp.exp(-q))
        f = f_ref[:, lanes].astype(jnp.float32)
        key = g_ref[:, lanes] / (1.0 + jnp.exp(f))
        logf = jnp.log1p(-key) + spike
        high = logf.astype(jnp.bfloat16)
        low = (logf - high.astype(jnp.float32)).astype(jnp.bfloat16)
        inside = jnp.dot(tri, high, preferred_element_type=jnp.float32) + jnp.dot(
            tri, low, preferred_element_type=jnp.float32
        )
        total = inside[rows - 1 : rows, :]
        kg = (key * jnp.exp(-inside)).astype(jnp.bfloat16)
        qd_ref[:, lanes] = (q * jnp.exp(inside)).astype(jnp.bfloat16)
        kg_ref[:, lanes] = kg
        v = val[:, pl.ds((at // width) * pair, pair)]
        state = lax.dot_general(v, kg, TN, preferred_element_type=jnp.float32)
        return total, state * jnp.exp(total)

    for h in range(heads):
        for g, (q_ref, f_ref, g_ref, k, qd, kg) in enumerate(
            ((qa, fa, ga, ka, qda, kga), (qb, fb, gb, kb, qdb, kgb))
        ):
            at = h * width + g * ka
            spike = bias[:, 2 * h + g : 2 * h + g + 1]
            total, state = prepare(q_ref, f_ref, g_ref, spike, k, h, qd, kg, at)
            high = total.astype(jnp.bfloat16)
            low = (total - high.astype(jnp.float32)).astype(jnp.bfloat16)
            msg[:dv, at : at + k] = state[g * dv : (g + 1) * dv].astype(jnp.bfloat16)
            first = lax.broadcasted_iota(jnp.int32, (16, k), 0) == 0
            msg[dv:, at : at + k] = jnp.where(first, high, low)

    pl.semaphore_wait(barrier, n_sp - 1)

    def copy_to(k):
        return pltpu.make_async_remote_copy(
            src_ref=msg, dst_ref=inbox.at[place], send_sem=send_sem.at[k],
            recv_sem=recv_sem.at[place], device_id={"sp": lax.rem(place + k, n_sp)},
            device_id_type=MESH_ID,
        )

    for k in range(1, n_sp):
        @pl.when(place + k < n_sp)
        def _():
            copy_to(k).start()

    lane = lax.broadcasted_iota(jnp.int32, (rows, pair), 1)

    def scored(qd, kg, v):
        scores = lax.dot_general(qd, kg, NT, preferred_element_type=jnp.float32)
        scores = jnp.where(causal, scores, 0.0).astype(jnp.bfloat16)
        return jnp.dot(scores, v, preferred_element_type=jnp.float32)

    for h in range(heads):
        v = val[:, h * pair : (h + 1) * pair]
        out_a = scored(qda[:, h * ka : (h + 1) * ka], kga[:, h * ka : (h + 1) * ka], v)
        out_b = scored(qdb[:, h * kb : (h + 1) * kb], kgb[:, h * kb : (h + 1) * kb], v)
        raw[:, h * pair : (h + 1) * pair] = jnp.where(lane < dv, out_a, out_b)

    carry[...] = jnp.zeros_like(carry)
    for j in range(n_sp - 1):
        @pl.when(j < place)
        def _():
            pltpu.make_async_remote_copy(
                src_ref=msg, dst_ref=inbox.at[j], send_sem=send_sem.at[0],
                recv_sem=recv_sem.at[j], device_id={"sp": place}, device_id_type=MESH_ID,
            ).wait_recv()
            total = inbox[j, dv : dv + 1, :].astype(jnp.float32) + inbox[
                j, dv + 1 : dv + 2, :
            ].astype(jnp.float32)
            carry[...] = jnp.exp(total) * carry[...] + inbox[j, :dv, :].astype(jnp.float32)

    gains = jnp.concatenate([gain[...], gain[...]], axis=1)
    for h in range(heads):
        c = carry[:, h * width : (h + 1) * width].astype(jnp.bfloat16)
        zero_a = jnp.zeros((dv, ka), jnp.bfloat16)
        zero_b = jnp.zeros((dv, kb), jnp.bfloat16)
        state_a = jnp.concatenate([c[:, :ka], zero_a], axis=0)
        state_b = jnp.concatenate([zero_b, c[:, ka:]], axis=0)
        cols = slice(h * pair, (h + 1) * pair)
        x = raw[:, cols]
        x = x + lax.dot_general(
            qda[:, h * ka : (h + 1) * ka], state_a, NT, preferred_element_type=jnp.float32
        )
        x = x + lax.dot_general(
            qdb[:, h * kb : (h + 1) * kb], state_b, NT, preferred_element_type=jnp.float32
        )
        squares = x * x
        sum_a = jnp.sum(jnp.where(lane < dv, squares, 0.0), axis=1, keepdims=True)
        sum_b = jnp.sum(jnp.where(lane < dv, 0.0, squares), axis=1, keepdims=True)
        scale = lax.rsqrt(jnp.where(lane < dv, sum_a, sum_b) * (1.0 / dv) + EPSILON)
        open_gate = 1.0 / (1.0 + jnp.exp(-gate[:, cols].astype(jnp.float32)))
        out[:, cols] = (x * scale * gains * open_gate).astype(jnp.bfloat16)

    for k in range(1, n_sp):
        @pl.when(place + k < n_sp)
        def _():
            copy_to(k).wait_send()


def mixer(qa, fa, ga, qb, fb, gb, val, gate, bias, gain):
    n_sp = lax.axis_size("sp")
    rows = qa.shape[0]
    heads = bias.shape[1] // 2
    ka, kb = qa.shape[1] // heads, qb.shape[1] // heads
    dv = gain.shape[0]
    width = ka + kb
    bf, f32 = jnp.bfloat16, jnp.float32
    vm = pl.BlockSpec(memory_space=pltpu.VMEM)
    return pl.pallas_call(
        functools.partial(mixer_kernel, n_sp, heads, ka, kb, dv),
        out_shape=jax.ShapeDtypeStruct(val.shape, bf),
        in_specs=[vm] * 10,
        out_specs=vm,
        scratch_shapes=[
            pltpu.VMEM((dv + 16, heads * width), bf),
            pltpu.VMEM((n_sp, dv + 16, heads * width), bf),
            pltpu.VMEM((dv, heads * width), f32),
            pltpu.VMEM(qa.shape, bf),
            pltpu.VMEM(qb.shape, bf),
            pltpu.VMEM(qa.shape, bf),
            pltpu.VMEM(qb.shape, bf),
            pltpu.VMEM(val.shape, f32),
            pltpu.SemaphoreType.DMA((n_sp,)),
            pltpu.SemaphoreType.DMA((n_sp,)),
        ],
        compiler_params=pltpu.CompilerParams(
            collective_id=0, has_side_effects=True, vmem_limit_bytes=48 << 20
        ),
        name="mixer",
    )(qa, fa, ga.reshape(1, -1), qb, fb, gb.reshape(1, -1), val, gate, bias, gain.reshape(1, -1))


def expert_rows(
    piece, dispatcher_columns, switch_matrix, expansion_matrix, contraction_matrix, member
):
    flat_rows = piece.reshape(-1, piece.shape[-1])
    scores = jax.nn.sigmoid(
        jnp.dot(flat_rows, dispatcher_columns, preferred_element_type=jnp.float32)
    )
    weights = scores / jnp.sum(scores, axis=1, keepdims=True)
    picked = (
        lax.broadcasted_iota(jnp.int32, (1, dispatcher_columns.shape[1]), 1) == member
    ).astype(jnp.float32)
    member_weight = jnp.sum(weights * picked, axis=1, keepdims=True)
    gate_proj = jnp.dot(flat_rows, switch_matrix[0], preferred_element_type=jnp.float32)
    up_proj = jnp.dot(flat_rows, expansion_matrix[0], preferred_element_type=jnp.float32)
    hidden = (jax.nn.silu(gate_proj) * up_proj).astype(jnp.bfloat16)
    product = jnp.dot(hidden, contraction_matrix[0], preferred_element_type=jnp.float32)
    return (member_weight * product).astype(jnp.bfloat16).reshape(piece.shape)


def shards(
    ask_preactivation_left,
    keep_preactivation_left,
    keep_bound_complement_left,
    ask_preactivation_right,
    keep_preactivation_right,
    keep_bound_complement_right,
    payload_entries,
    emission_switch_logits,
    added_log_keep_bias,
    lanewise_rescale,
    emission_matrix_alpha,
    emission_matrix_beta,
    skip_stream,
    postrecurrence_rescale,
    premixture_rescale,
    postmixture_rescale,
    dispatcher_columns,
    switch_matrix,
    expansion_matrix,
    contraction_matrix,
    item_specialist_cluster,
):
    heads = mixer(
        ask_preactivation_left,
        keep_preactivation_left,
        keep_bound_complement_left,
        ask_preactivation_right,
        keep_preactivation_right,
        keep_bound_complement_right,
        payload_entries,
        emission_switch_logits,
        added_log_keep_bias,
        lanewise_rescale,
    )
    row_count = skip_stream.shape[0]
    value_width = lanewise_rescale.shape[0]
    weights = jnp.stack(
        [
            emission_matrix_alpha.reshape(-1, value_width, skip_stream.shape[1]),
            emission_matrix_beta.reshape(-1, value_width, skip_stream.shape[1]),
        ],
        axis=1,
    ).reshape(-1, skip_stream.shape[1])
    term = jnp.dot(heads, weights, preferred_element_type=jnp.float32)
    mixed = lax.psum_scatter(
        lax.optimization_barrier(term.astype(jnp.bfloat16))
        .astype(jnp.float32)
        .astype(jnp.bfloat16),
        "tp",
        scatter_dimension=0,
        tiled=True,
    ).astype(jnp.float32)
    h_mid = (skip_stream.astype(jnp.float32) + rms_scale(mixed, postrecurrence_rescale)).astype(
        jnp.bfloat16
    )
    normed = rms_scale(h_mid.astype(jnp.float32), premixture_rescale).astype(jnp.bfloat16)
    groups = lax.axis_size("sp")
    capacity = (9 * row_count + 8 * groups - 1) // (8 * groups)
    member = item_specialist_cluster[:, None] == lax.broadcasted_iota(
        jnp.int32, (row_count, groups), 1
    )
    member_count = member.astype(jnp.int32)
    slot_rank = jnp.sum(jnp.cumsum(member_count, axis=0) * member_count, axis=1) - 1
    slot_id = item_specialist_cluster * capacity + slot_rank
    placing = (
        slot_id[None, :] == lax.broadcasted_iota(jnp.int32, (groups * capacity, row_count), 0)
    ).astype(jnp.bfloat16)
    outgoing = jnp.dot(placing, normed, preferred_element_type=jnp.float32).astype(jnp.bfloat16)
    outgoing = outgoing.reshape(groups, capacity, normed.shape[1])
    incoming = lax.all_to_all(outgoing, "sp", split_axis=0, concat_axis=0, tiled=True)
    own_member = lax.axis_index("tp") * switch_matrix.shape[2] // FF
    partials = expert_rows(
        lax.all_gather(incoming, "tp", axis=0, tiled=True),
        dispatcher_columns,
        switch_matrix,
        expansion_matrix,
        contraction_matrix,
        own_member,
    )
    summed = lax.psum_scatter(
        partials.astype(jnp.float32).astype(jnp.bfloat16), "tp", scatter_dimension=0, tiled=True
    )
    returned = lax.all_to_all(summed, "sp", split_axis=0, concat_axis=0, tiled=True)
    routed = jnp.einsum(
        "sr,sd->rd",
        placing,
        returned.reshape(groups * capacity, -1),
        preferred_element_type=jnp.float32,
    )
    return (h_mid.astype(jnp.float32) + rms_scale(routed, postmixture_rescale)).astype(jnp.bfloat16)


def solution(mesh):
    placed = (
        P("sp", "tp"),
        P("sp", "tp"),
        P("tp"),
        P("sp", "tp"),
        P("sp", "tp"),
        P("tp"),
        P("sp", "tp"),
        P("sp", "tp"),
        P("sp", "tp"),
        P(),
        P("tp", None),
        P("tp", None),
        P(("sp", "tp"), None),
        P(),
        P(),
        P(),
        P(None, "sp"),
        P("sp", None, "tp"),
        P("sp", None, "tp"),
        P("sp", "tp", None),
        P(("sp", "tp")),
    )
    return jax.shard_map(
        shards, mesh=mesh, in_specs=placed, out_specs=P(("sp", "tp"), None), check_vma=False
    )
```

time: 291 us -> 189 us (0.65)
  blocking collectives: 55.3 us -> 20.2 us
  other arithmetic: 29.6 us -> 5.04 us
  local copies, waits for them, and re-layouts: 34 us -> 9.93 us
  matrix products: 30.1 us -> 16 us
  waiting for transfers between devices: 126 us -> 114 us
  Pallas kernels: 0 us -> 9.85 us
    all_gather x4 -> x0, blocking collectives: 35.2 us -> none  [carried_in(): lax.all_gather(a.astype(kind), axis)]
    dot_general x10 -> x1, matrix products: 17.1 us -> 2.05 us  [shards(): term = jnp.dot(heads, weights, preferred_element_type=jnp.float32)]
    mul x6 -> x0, other arithmetic: 14.4 us -> none  [the longest x2 6.56 us: block_step(): k_grown = incoming_key_rows * jnp.exp(-inside)]
    reduce_scatter x1, waiting for transfers between devices: 51.2 us -> 39.3 us  [shards(): lax.psum_scatter(lax.optimization_barrier(term.astype(jnp.bfloat16)).asty...]
    unnamed x58 -> x35, local copies, waits for them, and re-layouts: 11.2 us -> 1.13 us
    pallas_call x0 -> x1, Pallas kernels: none -> 9.85 us  [mixer(): pl.pallas_call(functools.partial(mixer_kernel, n_sp, heads, ka, kb, dv),...]
    reshape x5 -> x0, local copies, waits for them, and re-layouts: 6.72 us -> none  [the longest x4 6.7 us: group_preparation(): jax.nn.sigmoid(-forget_gate.astype(jnp.float32)).reshape(block_shape)]
    add x2 -> x0, other arithmetic: 4.61 us -> none  [group_preparation(): jnp.log1p(-incoming_key_rows)]
where the time goes in v1:
time: 189 us
  waiting for transfers between devices  114 us (60%)
  blocking collectives  20.2 us (11%)
  matrix products  16 us (8%)
  between operations  13.4 us (7%)
  local copies, waits for them, and re-layouts  9.93 us (5%)
  Pallas kernels  9.85 us (5%)
  other arithmetic  5.04 us (3%)
    reduce_scatter x1, waiting for transfers between devices, shards(): lax.psum_scatter(partials.astype(jnp.float32).astype(jnp.bfloat16), 'tp',...  39.4 us
    reduce_scatter x1, waiting for transfers between devices, shards(): lax.psum_scatter(lax.optimization_barrier(term.astype(jnp.bfloat16)).asty...  39.3 us
    all_gather x1, waiting for transfers between devices, shards(): lax.all_gather(incoming, 'tp', axis=0, tiled=True)  35.5 us
    all_to_all x1, blocking collectives, shards(): lax.all_to_all(outgoing, 'sp', split_axis=0, concat_axis=0, tiled=True)  10.1 us
    all_to_all x1, blocking collectives, shards(): lax.all_to_all(summed, 'sp', split_axis=0, concat_axis=0, tiled=True)  10.1 us
    pallas_call x1, Pallas kernels, mixer(): pl.pallas_call(functools.partial(mixer_kernel, n_sp, heads, ka, kb, dv),...  9.85 us
    dot_general x1, matrix products, expert_rows(): jnp.dot(hidden, contraction_matrix[0], preferred_element_type=jnp.float32)  6.72 us
    reshape x1, local copies, waits for them, and re-layouts, expert_rows(): flat_rows = piece.reshape(-1, piece.shape[-1])  4.32 us
  transfers between devices with their start and end apart: 3, of which 3 were waited for; matrix products, arithmetic and copies ran while one was open for 0% of the time, Pallas kernels for 0%

profile of v1, /device:TPU:0, one launch (start us, length us, event | category | flops | bytes accessed | tf_op | source)
XLA Modules:
  0.0 188.8 jit_solution(8913509893585644611)
XLA Ops:
  6.6 1.0 copy.24.bias
  7.6 1.4 pad_maximum_fusion
  9.2 9.8 %mixer.1 = bf16[512,256]{1,0:T(8,128)(2,1)S(1)} custom-call(bf16[512,256]{1,0:T(8,128)(2,1)S(1)} %copy-done.3, bf16[512,256]{1,0:T(8,128)(2,1)S(1)} %copy-done.4, f32[1,256]{1,0:T(1,128)S(1)} %bitcast.29, bf16[512,512]{1,0:T(8,128)(2,1)S(1)} %copy-done.1, bf16[512,512]{1,0:T(8,128)(2,1)S(1)} %copy-done.2, f32[1,512]{1,0:T(1,128)S(1)} %bitcast.28, ...), custom_call_target="tpu_custom_call" | custom-call | tf_op jit(solution)/shard_map/mixer/pallas_call | solution.py:155
  19.0 2.1 %convolution_convert_fusion = bf16[512,2048]{1,0:T(8,128)(2,1)} fusion(bf16[512,256]{1,0:T(8,128)(2,1)S(1)} %mixer.1, bf16[256,2048]{1,0:T(8,128)(2,1)S(1)} %bitcast.31), kind=kOutput, calls=%fused_computation.1 | convolution fusion | flops 537919488 | bytes 3407872 | tf_op jit(solution)/shard_map/dot_general | solution.py:242
  21.3 0.1 reduce_window_sum.11
  21.4 0.2 select_reduce_fusion
  21.6 39.3 %reduce-scatter.3.cloned.1.call-done = bf16[64,2048]{1,0:T(8,128)(2,1)} async-done(((bf16[512,2048]{1,0:T(8,128)(2,1)}), bf16[64,2048]{1,0:T(8,128)(2,1)}) %reduce-scatter.3.cloned.1.call-update) | async-done | bytes 262160 | tf_op jit(solution)/shard_map/reduce_scatter | solution.py:243
  60.8 1.1 fusion.16
  62.0 1.2 fusion.20
  63.3 0.3 convolution_convert_fusion.1
  63.6 0.1 reshape.66
  63.7 10.1 %all_to_all.10 = bf16[4,18,2048]{2,1,0:T(8,128)(2,1)} all-to-all(bf16[4,18,2048]{2,1,0:T(8,128)(2,1)S(1)} %reshape.66), channel_id=1, replica_groups=mesh['sp'=4,'tp'=8] {'sp'}, dimensions={0} | all-to-all | bytes 589824 | tf_op jit(solution)/shard_map/all_to_all | solution.py:268
  73.9 35.5 %all-gather.2.cloned.1.call-done = bf16[32,18,2048]{2,1,0:T(8,128)(2,1)} async-done(((bf16[4,18,2048]{2,1,0:T(8,128)(2,1)}), bf16[32,18,2048]{2,1,0:T(8,128)(2,1)}) %all-gather.2.cloned.1.call-update) | async-done | bytes 2359312 | tf_op jit(solution)/shard_map/all_gather | solution.py:271
  109.4 4.3 %reshape.67 = bf16[576,2048]{1,0:T(8,128)(2,1)} reshape(bf16[32,18,2048]{2,1,0:T(8,128)(2,1)} %all-gather.2.cloned.1.call-done) | data formatting | bytes 4718592 | tf_op jit(solution)/shard_map/reshape | solution.py:182
  113.7 2.5 %divide_reduce_fusion = (f32[576]{0:T(1024)S(1)}, f32[576,2]{0,1:T(2,128)S(1)}) fusion(bf16[576,2048]{1,0:T(8,128)(2,1)} %reshape.67, bf16[2048,2]{0,1:T(2,128)(2,1)S(1)} %copy-done.14), kind=kOutput, calls=%fused_computation.39 | convolution fusion | flops 4722624 | bytes 2374400 | tf_op jit(solution)/shard_map/dot_general | solution.py:184
  116.3 4.0 %fusion.3 = f32[576,512]{1,0:T(8,128)} fusion(bf16[576,2048]{1,0:T(8,128)(2,1)S(1)} %copy-done.10, bf16[1,2048,512]{2,1,0:T(8,128)(2,1)} %param.38), kind=kOutput, calls=%fused_computation.6 | convolution fusion | flops 1207959552 | bytes 5636096 | tf_op jit(solution)/shard_map/dot_general | solution.py:191
  120.3 0.1 multiply_reduce_fusion.1
  120.4 6.7 %multiply_convert_fusion = bf16[576,2048]{1,0:T(8,128)(2,1)} fusion(f32[576]{0:T(1024)S(1)} %multiply_reduce_fusion.1, bf16[1,512,2048]{2,1,0:T(8,128)(2,1)S(1)} %copy-done, bf16[576,2048]{1,0:T(8,128)(2,1)} %reshape.67, bf16[1,2048,512]{2,1,0:T(8,128)(2,1)} %param.39, f32[576,512]{1,0:T(8,128)} %fusion.3), kind=kOutput, calls=%fused_computation | convolution fusion | flops 2420047872 | bytes 10094848 | tf_op jit(solution)/shard_map/dot_general | solution.py:194
  127.1 4.3 %reshape.68 = bf16[32,18,2048]{2,1,0:T(8,128)(2,1)} reshape(bf16[576,2048]{1,0:T(8,128)(2,1)} %multiply_convert_fusion) | data formatting | bytes 4718592 | tf_op jit(solution)/shard_map/reshape | solution.py:195
  131.4 39.4 %reduce-scatter.5.cloned.1.call-done = bf16[4,18,2048]{2,1,0:T(8,128)(2,1)} async-done(((bf16[32,18,2048]{2,1,0:T(8,128)(2,1)}), bf16[4,18,2048]{2,1,0:T(8,128)(2,1)}) %reduce-scatter.5.cloned.1.call-update) | async-done | bytes 294928 | tf_op jit(solution)/shard_map/reduce_scatter | solution.py:278
  170.8 10.1 %all_to_all.11 = bf16[4,18,2048]{2,1,0:T(8,128)(2,1)S(1)} all-to-all(bf16[4,18,2048]{2,1,0:T(8,128)(2,1)} %reduce-scatter.5.cloned.1.call-done), channel_id=1, replica_groups=mesh['sp'=4,'tp'=8] {'sp'}, dimensions={0} | all-to-all | bytes 589824 | tf_op jit(solution)/shard_map/all_to_all | solution.py:281
  180.9 0.1 reshape.69
  181.0 0.4 multiply_reduce_fusion
  181.4 0.9 fusion.23
  (46 shorter events, 0.4 us)
Async XLA Ops:
  6.5 113.8 %copy-start = (bf16[1,512,2048]{2,1,0:T(8,128)(2,1)S(1)}, bf16[1,512,2048]{2,1,0:T(8,128)(2,1)}, u32[]{:S(2)}) copy-start(bf16[1,512,2048]{2,1,0:T(8,128)(2,1)} %param.40) | copy-start | bytes 6291460
  6.5 2.5 %copy-start.9 = (f32[64]{0:T(128)S(1)}, f32[64]{0:T(128)}, u32[]{:S(2)}) copy-start(f32[64]{0:T(128)} %param.30) | copy-start | bytes 772
  6.5 2.5 %copy-start.7 = (f32[512]{0:T(512)S(1)}, f32[512]{0:T(512)}, u32[]{:S(2)}) copy-start(f32[512]{0:T(512)} %param.26) | copy-start | bytes 6148
  6.5 2.5 %copy-start.2 = (bf16[512,512]{1,0:T(8,128)(2,1)S(1)}, bf16[512,512]{1,0:T(8,128)(2,1)}, u32[]{:S(2)}) copy-start(bf16[512,512]{1,0:T(8,128)(2,1)} %fb.1) | copy-start | bytes 1572868
  6.5 2.5 %copy-start.1 = (bf16[512,512]{1,0:T(8,128)(2,1)S(1)}, bf16[512,512]{1,0:T(8,128)(2,1)}, u32[]{:S(2)}) copy-start(bf16[512,512]{1,0:T(8,128)(2,1)} %qb.1) | copy-start | bytes 1572868
  6.5 2.5 %copy-start.8 = (f32[256]{0:T(256)S(1)}, f32[256]{0:T(256)}, u32[]{:S(2)}) copy-start(f32[256]{0:T(256)} %param.23) | copy-start | bytes 3076
  6.6 54.3 %reduce-scatter.3.cloned.1.call-start = ((), (), s32[]{:S(2)}) async-start(), calls=%async_computation.4 | async-start | bytes 2359296 | tf_op jit(solution)/shard_map/reduce_scatter | solution.py:243
  7.6 1.5 copy-start.3
  7.6 1.5 copy-start.4
  7.6 1.5 copy-start.5
  7.6 1.5 copy-start.6
  19.0 2.1 %copy-start.16 = (s32[64]{0:T(128)S(1)}, s32[64]{0:T(128)}, u32[]{:S(2)}) copy-start(s32[64]{0:T(128)} %param.41) | copy-start | bytes 772
  21.1 40.9 %copy-start.11 = (bf16[64,2048]{1,0:T(8,128)(2,1)S(1)}, bf16[64,2048]{1,0:T(8,128)(2,1)}, u32[]{:S(2)}) copy-start(bf16[64,2048]{1,0:T(8,128)(2,1)} %param.33) | copy-start | bytes 786436
  21.1 40.9 %copy-start.12 = (f32[2048]{0:T(1024)S(1)}, f32[2048]{0:T(1024)}, u32[]{:S(2)}) copy-start(f32[2048]{0:T(1024)} %param.34) | copy-start | bytes 24580
  21.1 42.1 %copy-start.13 = (f32[2048]{0:T(1024)S(1)}, f32[2048]{0:T(1024)}, u32[]{:S(2)}) copy-start(f32[2048]{0:T(1024)} %param.35) | copy-start | bytes 24580
  21.1 88.2 %all-gather.2.cloned.1.call-start = ((), (), s32[]{:S(2)}) async-start(), calls=%async_computation.5 | async-start | bytes 3538944 | tf_op jit(solution)/shard_map/all_gather | solution.py:271
  73.8 97.1 %reduce-scatter.5.cloned.1.call-start = ((), (), s32[]{:S(2)}) async-start(), calls=%async_computation.6 | async-start | bytes 3538944 | tf_op jit(solution)/shard_map/reduce_scatter | solution.py:278
  73.9 39.8 %copy-start.14 = (bf16[2048,2]{0,1:T(2,128)(2,1)S(1)}, bf16[2048,2]{0,1:T(2,128)(2,1)}, u32[]{:S(2)}) copy-start(bf16[2048,2]{0,1:T(2,128)(2,1)} %param.37) | copy-start | bytes 24580
  113.7 2.6 %copy-start.10 = (bf16[576,2048]{1,0:T(8,128)(2,1)S(1)}, bf16[576,2048]{1,0:T(8,128)(2,1)}, u32[]{:S(2)}) copy-start(bf16[576,2048]{1,0:T(8,128)(2,1)} %reshape.67) | copy-start | bytes 7077892
  131.4 50.0 %copy-start.15 = (f32[2048]{0:T(1024)S(1)}, f32[2048]{0:T(1024)}, u32[]{:S(2)}) copy-start(f32[2048]{0:T(1024)} %param.36) | copy-start | bytes 24580
Sparse Core Ops, SparseCore 0:
  21.2 39.5 reduce-scatter.2
  73.9 35.4 all-gather.1
  131.5 39.2 reduce-scatter.4

commit v2 on v1

--- a/solution.py
+++ b/solution.py
@@ -176,23 +176,398 @@
     )(qa, fa, ga.reshape(1, -1), qb, fb, gb.reshape(1, -1), val, gate, bias, gain.reshape(1, -1))
 
 
-def expert_rows(
-    piece, dispatcher_columns, switch_matrix, expansion_matrix, contraction_matrix, member
+def landed(ref, sem, source):
+    pltpu.make_async_remote_copy(
+        src_ref=ref, dst_ref=ref, send_sem=sem, recv_sem=sem, device_id=source,
+        device_id_type=MESH_ID,
+    ).wait_recv()
+
+
+def line_reduce(z, core, nz, rows, part, twin, box_r, box_l, out_r, out_l, sems, to_right, to_left):
+    twin_recv, send_r, recv_r, send_l, recv_l = sems
+    chunks = part.shape[1]
+    own = pl.ds(pl.multiple_of(core * rows, rows), rows)
+
+    def base(d, ch):
+        return part[d, ch, own, :].astype(jnp.float32) + twin[d, ch].astype(jnp.float32)
+
+    def twin_wait(d):
+        landed(twin.at[d], twin_recv.at[d], to_right)
+
+    def hop(out, box, send, recv, d, ch, to):
+        return pltpu.make_async_remote_copy(
+            src_ref=out.at[d, ch], dst_ref=box.at[d, ch], send_sem=send.at[d, ch],
+            recv_sem=recv.at[d, ch], device_id=to, device_id_type=MESH_ID,
+        )
+
+    def side(d, has_in, out, box, send, recv, to):
+        twin_wait(d)
+        for ch in range(chunks):
+            @pl.when(has_in)
+            def _():
+                hop(out, box, send, recv, d, ch, to).wait_recv()
+                total = base(d, ch) + box[d, ch].astype(jnp.float32)
+                out[d, ch] = total.astype(jnp.bfloat16)
+
+            @pl.when(jnp.logical_not(has_in))
+            def _():
+                out[d, ch] = base(d, ch).astype(jnp.bfloat16)
+
+            hop(out, box, send, recv, d, ch, to).start()
+
+    def step(tau, _):
+        @pl.when((tau >= z) & (z < nz - 1))
+        def _():
+            side(nz - 1 + z - tau, z > 0, out_r, box_r, send_r, recv_r, to_right)
+
+        @pl.when((tau + z >= nz - 1) & (z > 0))
+        def _():
+            side(tau + z - (nz - 1), z < nz - 1, out_l, box_l, send_l, recv_l, to_left)
+
+        return 0
+
+    lax.fori_loop(0, nz - 1, step, 0)
+
+    def finish(total):
+        twin_wait(z)
+        for ch in range(chunks):
+            total[ch] = base(z, ch)
+
+            @pl.when(z > 0)
+            def _():
+                hop(out_r, box_r, send_r, recv_r, z, ch, to_right).wait_recv()
+                total[ch] = total[ch] + box_r[z, ch].astype(jnp.float32)
+
+            @pl.when(z < nz - 1)
+            def _():
+                hop(out_l, box_l, send_l, recv_l, z, ch, to_left).wait_recv()
+                total[ch] = total[ch] + box_l[z, ch].astype(jnp.float32)
+
+    def drain():
+        def one(d, _):
+            for ch in range(chunks):
+                @pl.when(d > z)
+                def _():
+                    hop(out_r, box_r, send_r, recv_r, d, ch, to_right).wait_send()
+
+                @pl.when(d < z)
+                def _():
+                    hop(out_l, box_l, send_l, recv_l, d, ch, to_left).wait_send()
+
+            return 0
+
+        lax.fori_loop(0, nz, one, 0)
+
+    return finish, drain
+
+
+def experts_kernel(
+    dv, n_sp, nz, cap, pad,
+    heads, alpha, beta, skip, gain1, gain2, gain3, router, w1, w2, w3, cluster,
+    out,
+    wcat, w1v, w2v, w3v, part, twin, box_r, box_l, out_r, out_l, mixed, hmid, placing,
+    sp_out, sp_in, xs, part2, twin2, box_r2, box_l2, out_r2, out_l2, summed, back_out, back_in,
+    wsem, tw_s, tw_r, rs_sr, rs_rr, rs_sl, rs_rl, sp_s, sp_r,
+    ag_sr, ag_rr, ag_sl, ag_rl, ag_ds, ag_dr,
+    tw2_s, tw2_r, rs2_sr, rs2_rr, rs2_sl, rs2_rl, bk_s, bk_r,
 ):
-    flat_rows = piece.reshape(-1, piece.shape[-1])
-    scores = jax.nn.sigmoid(
-        jnp.dot(flat_rows, dispatcher_columns, preferred_element_type=jnp.float32)
-    )
-    weights = scores / jnp.sum(scores, axis=1, keepdims=True)
-    picked = (
-        lax.broadcasted_iota(jnp.int32, (1, dispatcher_columns.shape[1]), 1) == member
-    ).astype(jnp.float32)
-    member_weight = jnp.sum(weights * picked, axis=1, keepdims=True)
-    gate_proj = jnp.dot(flat_rows, switch_matrix[0], preferred_element_type=jnp.float32)
-    up_proj = jnp.dot(flat_rows, expansion_matrix[0], preferred_element_type=jnp.float32)
-    hidden = (jax.nn.silu(gate_proj) * up_proj).astype(jnp.bfloat16)
-    product = jnp.dot(hidden, contraction_matrix[0], preferred_element_type=jnp.float32)
-    return (member_weight * product).astype(jnp.bfloat16).reshape(piece.shape)
+    f32, bf = jnp.float32, jnp.bfloat16
+    place, t = lax.axis_index("sp"), lax.axis_index("tp")
+    z, core = t // 2, t % 2
+    peer = {"tp": z * 2 + 1 - core}
+    to_right = {"tp": jnp.minimum(z + 1, nz - 1) * 2 + core}
+    to_left = {"tp": jnp.maximum(z - 1, 0) * 2 + core}
+
+    barrier = pltpu.get_barrier_semaphore()
+    for k in range(1, n_sp):
+        pl.semaphore_signal(
+            barrier, inc=1, device_id={"sp": lax.rem(place + k, n_sp)}, device_id_type=MESH_ID
+        )
+    pl.semaphore_signal(barrier, inc=1, device_id=peer, device_id_type=MESH_ID)
+
+    @pl.when(z < nz - 1)
+    def _():
+        pl.semaphore_signal(barrier, inc=1, device_id=to_right, device_id_type=MESH_ID)
+
+    @pl.when(z > 0)
+    def _():
+        pl.semaphore_signal(barrier, inc=1, device_id=to_left, device_id_type=MESH_ID)
+
+    loads = [
+        pltpu.make_async_copy(src.at[0], dst, wsem.at[i])
+        for i, (src, dst) in enumerate(((w1, w1v), (w2, w2v), (w3, w3v)))
+    ]
+    for load in loads:
+        load.start()
+
+    rows, width = skip.shape
+    chunks = part.shape[1]
+    half = width // chunks
+    slots = n_sp * pad
+    compact = xs.shape[2] // 2
+    for h in range(alpha.shape[0] // dv):
+        wcat[2 * h * dv : (2 * h + 1) * dv] = alpha[h * dv : (h + 1) * dv]
+        wcat[(2 * h + 1) * dv : (2 * h + 2) * dv] = beta[h * dv : (h + 1) * dv]
+
+    pl.semaphore_wait(
+        barrier,
+        n_sp + jnp.where(z > 0, 1, 0) + jnp.where(z < nz - 1, 1, 0),
+    )
+
+    def twin_copy(src, dst, d, size, send, recv):
+        theirs = pl.ds(pl.multiple_of((1 - core) * size, size), size)
+        return pltpu.make_async_remote_copy(
+            src_ref=src.at[d, :, theirs, :], dst_ref=dst.at[d], send_sem=send.at[d],
+            recv_sem=recv.at[d], device_id=peer, device_id_type=MESH_ID,
+        )
+
+    def project(i, _):
+        d = jnp.where(i % 2 == 0, nz - 1 - i // 2, i // 2)
+        x = heads[pl.ds(pl.multiple_of(d * 2 * rows, 2 * rows), 2 * rows), :]
+        for ch in range(chunks):
+            part[d, ch] = jnp.dot(
+                x, wcat[:, ch * half : (ch + 1) * half], preferred_element_type=f32
+            ).astype(bf)
+        twin_copy(part, twin, d, rows, tw_s, tw_r).start()
+        return 0
+
+    lax.fori_loop(0, nz, project, 0)
+    finish, drain = line_reduce(
+        z, core, nz, rows, part, twin, box_r, box_l, out_r, out_l,
+        (tw_r, rs_sr, rs_rr, rs_sl, rs_rl), to_right, to_left,
+    )
+    finish(mixed)
+
+    def whole(ref):
+        return jnp.concatenate([ref[ch] for ch in range(chunks)], axis=1)
+
+    mid = skip[...].astype(f32) + rms_scale(whole(mixed), gain1[...])
+    hmid[...] = mid.astype(bf)
+    normed = rms_scale(hmid[...].astype(f32), gain2[...]).astype(bf)
+
+    group = cluster[...]
+    onehot = lax.broadcasted_iota(jnp.int32, (n_sp, rows), 0) == group
+    ones = jnp.where(onehot, 1.0, 0.0)
+    upto = jnp.where(
+        lax.broadcasted_iota(jnp.int32, (rows, rows), 0)
+        <= lax.broadcasted_iota(jnp.int32, (rows, rows), 1),
+        1.0,
+        0.0,
+    ).astype(bf)
+    counts = jnp.dot(ones.astype(bf), upto, preferred_element_type=f32)
+    rank = jnp.sum(ones * counts, axis=0, keepdims=True).astype(jnp.int32) - 1
+    slot = group * pad + rank
+    placing[...] = jnp.where(
+        lax.broadcasted_iota(jnp.int32, (slots, rows), 0) == slot, 1.0, 0.0
+    ).astype(bf)
+    col = lax.broadcasted_iota(jnp.int32, (compact, slots), 1)
+    inner = col & (pad - 1)
+    target = (col >> (pad.bit_length() - 1)) * cap + inner
+    packing = jnp.where(
+        (lax.broadcasted_iota(jnp.int32, (compact, slots), 0) == target) & (inner < cap), 1.0, 0.0
+    ).astype(bf)
+
+    def sp_copy(src, dst, k, send, recv):
+        g = lax.rem(place + k, n_sp)
+        return pltpu.make_async_remote_copy(
+            src_ref=src.at[g], dst_ref=dst.at[place], send_sem=send.at[g],
+            recv_sem=recv.at[place], device_id={"sp": g}, device_id_type=MESH_ID,
+        )
+
+    def sp_exchange(src, dst, send, recv):
+        for k in range(1, n_sp):
+            sp_copy(src, dst, k, send, recv).start()
+        dst[place] = src[place]
+        for k in range(1, n_sp):
+            g = lax.rem(place + k, n_sp)
+            landed(dst.at[g], recv.at[g], peer)
+
+    sp_out[...] = (
+        jnp.dot(placing[...], normed, preferred_element_type=f32)
+        .astype(bf)
+        .reshape(n_sp, pad, width)
+    )
+    sp_exchange(sp_out, sp_in, sp_s, sp_r)
+    packed = jnp.dot(
+        packing, sp_in[...].reshape(slots, width), preferred_element_type=f32
+    ).astype(bf)
+    mine = pl.ds(pl.multiple_of(core * compact, compact), compact)
+    theirs = pl.ds(pl.multiple_of((1 - core) * compact, compact), compact)
+    for ch in range(chunks):
+        xs[z, ch, mine, :] = packed[:, ch * half : (ch + 1) * half]
+
+    for load in loads:
+        load.wait()
+
+    def spread(d, ch, send, recv, to):
+        return pltpu.make_async_remote_copy(
+            src_ref=xs.at[d, ch, mine, :], dst_ref=xs.at[d, ch, mine, :],
+            send_sem=send.at[d, ch], recv_sem=recv.at[d, ch], device_id=to,
+            device_id_type=MESH_ID,
+        )
+
+    member = t * w1v.shape[1] // FF
+
+    def expert(d):
+        for ch in range(chunks):
+            landed(xs.at[d, ch, theirs, :], ag_dr.at[d, ch], peer)
+        gate = up = score = 0.0
+        for ch in range(chunks):
+            x = xs[d, ch]
+            depth = pl.ds(ch * half, half)
+            gate = gate + jnp.dot(x, w1v[depth, :], preferred_element_type=f32)
+            up = up + jnp.dot(x, w2v[depth, :], preferred_element_type=f32)
+            score = score + jnp.dot(x, router[depth, :], preferred_element_type=f32)
+        score = 1.0 / (1.0 + jnp.exp(-score))
+        picked = lax.broadcasted_iota(jnp.int32, score.shape, 1) == member
+        weight = jnp.sum(jnp.where(picked, score, 0.0), axis=1, keepdims=True) / jnp.sum(
+            score, axis=1, keepdims=True
+        )
+        hidden = (gate / (1.0 + jnp.exp(-gate)) * up).astype(bf)
+        for ch in range(chunks):
+            y = jnp.dot(hidden, w3v[:, ch * half : (ch + 1) * half], preferred_element_type=f32)
+            part2[d, ch] = (weight * y).astype(bf)
+        twin_copy(part2, twin2, d, compact, tw2_s, tw2_r).start()
+
+    def gather(tau, _):
+        low, high = z - tau, z + tau
+        for ch in range(chunks):
+            @pl.when(low >= 0)
+            def _():
+                @pl.when(tau > 0)
+                def _():
+                    spread(low, ch, ag_sr, ag_rr, to_right).wait_recv()
+
+                @pl.when(z < nz - 1)
+                def _():
+                    spread(low, ch, ag_sr, ag_rr, to_right).start()
+
+                spread(low, ch, ag_ds, ag_dr, peer).start()
+
+            @pl.when(high < nz)
+            def _():
+                @pl.when(tau > 0)
+                def _():
+                    spread(high, ch, ag_sl, ag_rl, to_left).wait_recv()
+
+                @pl.when(z > 0)
+                def _():
+                    spread(high, ch, ag_sl, ag_rl, to_left).start()
+
+                @pl.when(tau > 0)
+                def _():
+                    spread(high, ch, ag_ds, ag_dr, peer).start()
+
+        @pl.when(low >= 0)
+        def _():
+            expert(low)
+
+        @pl.when((high < nz) & (tau > 0))
+        def _():
+            expert(high)
+
+        return 0
+
+    lax.fori_loop(0, nz, gather, 0)
+    finish2, drain2 = line_reduce(
+        z, core, nz, compact, part2, twin2, box_r2, box_l2, out_r2, out_l2,
+        (tw2_r, rs2_sr, rs2_rr, rs2_sl, rs2_rl), to_right, to_left,
+    )
+    finish2(summed)
+    back_out[...] = (
+        lax.dot_general(packing, whole(summed).astype(bf), TN, preferred_element_type=f32)
+        .astype(bf)
+        .reshape(n_sp, pad, width)
+    )
+    sp_exchange(back_out, back_in, bk_s, bk_r)
+    routed = lax.dot_general(
+        placing[...], back_in[...].reshape(slots, width), TN, preferred_element_type=f32
+    )
+    out[...] = (hmid[...].astype(f32) + rms_scale(routed, gain3[...])).astype(bf)
+
+    drain()
+    drain2()
+
+    def settle(d, _):
+        twin_copy(part, twin, d, rows, tw_s, tw_r).wait_send()
+        twin_copy(part2, twin2, d, compact, tw2_s, tw2_r).wait_send()
+        for ch in range(chunks):
+            spread(d, ch, ag_ds, ag_dr, peer).wait_send()
+
+            @pl.when((d <= z) & (z < nz - 1))
+            def _():
+                spread(d, ch, ag_sr, ag_rr, to_right).wait_send()
+
+            @pl.when((d >= z) & (z > 0))
+            def _():
+                spread(d, ch, ag_sl, ag_rl, to_left).wait_send()
+
+        return 0
+
+    lax.fori_loop(0, nz, settle, 0)
+    for k in range(1, n_sp):
+        sp_copy(sp_out, sp_in, k, sp_s, sp_r).wait_send()
+        sp_copy(back_out, back_in, k, bk_s, bk_r).wait_send()
+
+
+def mixture(dv, heads, alpha, beta, skip, g1, g2, g3, router, w1, w2, w3, cluster):
+    n_sp, nz = lax.axis_size("sp"), lax.axis_size("tp") // 2
+    rows, width = skip.shape
+    cap = (9 * rows + 8 * n_sp - 1) // (8 * n_sp)
+    pad = 16
+    while pad < cap:
+        pad *= 2
+    compact = (n_sp * cap + 15) // 16 * 16
+    chunks, half = 2, width // 2
+    f32, bf = jnp.float32, jnp.bfloat16
+    vm = pl.BlockSpec(memory_space=pltpu.VMEM)
+    hbm = pl.BlockSpec(memory_space=pl.ANY)
+    line = (nz, chunks, rows, half)
+    line2 = (nz, chunks, compact, half)
+    dma = pltpu.SemaphoreType.DMA
+    reduce_sems = [dma((nz,))] * 2 + [dma((nz, chunks))] * 4
+    return pl.pallas_call(
+        functools.partial(experts_kernel, dv, n_sp, nz, cap, pad),
+        out_shape=jax.ShapeDtypeStruct(skip.shape, bf),
+        in_specs=[vm] * 8 + [hbm] * 3 + [vm],
+        out_specs=vm,
+        scratch_shapes=[
+            pltpu.VMEM((2 * alpha.shape[0], width), bf),
+            pltpu.VMEM(w1.shape[1:], bf),
+            pltpu.VMEM(w2.shape[1:], bf),
+            pltpu.VMEM(w3.shape[1:], bf),
+            pltpu.VMEM((nz, chunks, 2 * rows, half), bf),
+        ]
+        + [pltpu.VMEM(line, bf)] * 5
+        + [
+            pltpu.VMEM(line[1:], f32),
+            pltpu.VMEM(skip.shape, bf),
+            pltpu.VMEM((n_sp * pad, rows), bf),
+            pltpu.VMEM((n_sp, pad, width), bf),
+            pltpu.VMEM((n_sp, pad, width), bf),
+            pltpu.VMEM((nz, chunks, 2 * compact, half), bf),
+            pltpu.VMEM((nz, chunks, 2 * compact, half), bf),
+        ]
+        + [pltpu.VMEM(line2, bf)] * 5
+        + [
+            pltpu.VMEM(line2[1:], f32),
+            pltpu.VMEM((n_sp, pad, width), bf),
+            pltpu.VMEM((n_sp, pad, width), bf),
+            dma((3,)),
+        ]
+        + reduce_sems
+        + [dma((n_sp,))] * 2
+        + [dma((nz, chunks))] * 6
+        + reduce_sems
+        + [dma((n_sp,))] * 2,
+        compiler_params=pltpu.CompilerParams(
+            collective_id=1, has_side_effects=True, vmem_limit_bytes=60 << 20
+        ),
+        name="mixture",
+    )(
+        heads, alpha, beta, skip, g1.reshape(1, -1), g2.reshape(1, -1), g3.reshape(1, -1),
+        router, w1, w2, w3, cluster.reshape(1, -1),
+    )
 
 
 def shards(
@@ -230,62 +605,21 @@
         added_log_keep_bias,
         lanewise_rescale,
     )
-    row_count = skip_stream.shape[0]
-    value_width = lanewise_rescale.shape[0]
-    weights = jnp.stack(
-        [
-            emission_matrix_alpha.reshape(-1, value_width, skip_stream.shape[1]),
-            emission_matrix_beta.reshape(-1, value_width, skip_stream.shape[1]),
-        ],
-        axis=1,
-    ).reshape(-1, skip_stream.shape[1])
-    term = jnp.dot(heads, weights, preferred_element_type=jnp.float32)
-    mixed = lax.psum_scatter(
-        lax.optimization_barrier(term.astype(jnp.bfloat16))
-        .astype(jnp.float32)
-        .astype(jnp.bfloat16),
-        "tp",
-        scatter_dimension=0,
-        tiled=True,
-    ).astype(jnp.float32)
-    h_mid = (skip_stream.astype(jnp.float32) + rms_scale(mixed, postrecurrence_rescale)).astype(
-        jnp.bfloat16
-    )
-    normed = rms_scale(h_mid.astype(jnp.float32), premixture_rescale).astype(jnp.bfloat16)
-    groups = lax.axis_size("sp")
-    capacity = (9 * row_count + 8 * groups - 1) // (8 * groups)
-    member = item_specialist_cluster[:, None] == lax.broadcasted_iota(
-        jnp.int32, (row_count, groups), 1
-    )
-    member_count = member.astype(jnp.int32)
-    slot_rank = jnp.sum(jnp.cumsum(member_count, axis=0) * member_count, axis=1) - 1
-    slot_id = item_specialist_cluster * capacity + slot_rank
-    placing = (
-        slot_id[None, :] == lax.broadcasted_iota(jnp.int32, (groups * capacity, row_count), 0)
-    ).astype(jnp.bfloat16)
-    outgoing = jnp.dot(placing, normed, preferred_element_type=jnp.float32).astype(jnp.bfloat16)
-    outgoing = outgoing.reshape(groups, capacity, normed.shape[1])
-    incoming = lax.all_to_all(outgoing, "sp", split_axis=0, concat_axis=0, tiled=True)
-    own_member = lax.axis_index("tp") * switch_matrix.shape[2] // FF
-    partials = expert_rows(
-        lax.all_gather(incoming, "tp", axis=0, tiled=True),
+    return mixture(
+        lanewise_rescale.shape[0],
+        heads,
+        emission_matrix_alpha,
+        emission_matrix_beta,
+        skip_stream,
+        postrecurrence_rescale,
+        premixture_rescale,
+        postmixture_rescale,
         dispatcher_columns,
         switch_matrix,
         expansion_matrix,
         contraction_matrix,
-        own_member,
-    )
-    summed = lax.psum_scatter(
-        partials.astype(jnp.float32).astype(jnp.bfloat16), "tp", scatter_dimension=0, tiled=True
-    )
-    returned = lax.all_to_all(summed, "sp", split_axis=0, concat_axis=0, tiled=True)
-    routed = jnp.einsum(
-        "sr,sd->rd",
-        placing,
-        returned.reshape(groups * capacity, -1),
-        preferred_element_type=jnp.float32,
-    )
-    return (h_mid.astype(jnp.float32) + rms_scale(routed, postmixture_rescale)).astype(jnp.bfloat16)
+        item_specialist_cluster,
+    )
 
 
 def solution(mesh):

time: 189 us -> 118 us (0.62)
  waiting for transfers between devices: 114 us -> 0 us
  Pallas kernels: 9.85 us -> 105 us
  blocking collectives: 20.2 us -> 0 us
  matrix products: 16 us -> 0 us
  between operations: 13.4 us -> 0.05 us
  other arithmetic: 5.04 us -> 0 us
  local copies, waits for them, and re-layouts: 9.93 us -> 12.2 us
    pallas_call x0 -> x1, Pallas kernels: none -> 95.1 us  [mixture(): pl.pallas_call(functools.partial(experts_kernel, dv, n_sp, nz, cap, pad),...]
    reduce_scatter x2 -> x0, waiting for transfers between devices: 78.7 us -> none  [the longest x1 39.4 us: shards(): lax.psum_scatter(partials.astype(jnp.float32).astype(jnp.bfloat16), 'tp',...]
    all_gather x1 -> x0, waiting for transfers between devices: 35.5 us -> none  [shards(): lax.all_gather(incoming, 'tp', axis=0, tiled=True)]
    all_to_all x2 -> x0, blocking collectives: 20.2 us -> none  [the longest x1 10.1 us: shards(): lax.all_to_all(outgoing, 'sp', split_axis=0, concat_axis=0, tiled=True)]
    dot_general x6 -> x0, matrix products: 16 us -> none  [the longest x1 6.72 us: expert_rows(): jnp.dot(hidden, contraction_matrix[0], preferred_element_type=jnp.float32)]
    unnamed x35 -> x25, local copies, waits for them, and re-layouts: 1.13 us -> 12.2 us
    reshape x4 -> x0, local copies, waits for them, and re-layouts: 8.8 us -> none  [the longest x1 4.32 us: expert_rows(): flat_rows = piece.reshape(-1, piece.shape[-1])]
    reduce_sum x4 -> x0, other arithmetic: 2.6 us -> none  [the longest x2 2.35 us: rms_scale(): jnp.mean(features * features, axis=-1, keepdims=True) + EPSILON]
  transfers between devices with their start and end apart: 3 -> 0, of which waited for: 3 -> 0; matrix products, arithmetic and copies ran while one was open for 0% -> 0% of each run, Pallas kernels for 0% -> 0%
where the time goes in v2:
time: 118 us; the launch traced here: 117 us
  Pallas kernels  105 us (89%)
  local copies, waits for them, and re-layouts  12.2 us (10%)
    pallas_call x1, Pallas kernels, mixture(): pl.pallas_call(functools.partial(experts_kernel, dv, n_sp, nz, cap, pad),...  95.1 us
    unnamed x25, local copies, waits for them, and re-layouts  12.2 us
    pallas_call x1, Pallas kernels, mixer(): pl.pallas_call(functools.partial(mixer_kernel, n_sp, heads, ka, kb, dv),...  9.83 us

profile of v2, /device:TPU:0, one launch (start us, length us, event | category | flops | bytes accessed | tf_op | source)
XLA Modules:
  0.0 117.1 jit_solution(12328223070423123471)
XLA Ops:
  0.0 0.0 copy-start.10
  0.0 0.8 copy.22.bias
  0.9 0.0 copy-start.1
  0.9 1.0 copy-done.1
  1.9 0.0 copy-start.2
  1.9 1.0 copy-done.2
  2.9 0.0 copy-start.3
  3.0 0.9 copy-done.3
  3.9 0.0 copy-start.4
  3.9 0.9 copy-done.4
  4.8 0.0 copy-start.5
  4.9 0.9 copy-done.5
  5.8 0.0 copy-start.6
  5.8 0.9 copy-done.6
  6.8 0.7 copy-done.7
  7.4 0.7 copy-done.8
  8.1 0.7 copy-done.9
  8.8 9.8 %mixer.1.heads = bf16[512,256]{1,0:T(8,128)(2,1)S(1)} custom-call(bf16[512,256]{1,0:T(8,128)(2,1)S(1)} %copy-done.3, bf16[512,256]{1,0:T(8,128)(2,1)S(1)} %copy-done.4, f32[1,256]{1,0:T(1,128)S(1)} %bitcast.8, bf16[512,512]{1,0:T(8,128)(2,1)S(1)} %copy-done.1, bf16[512,512]{1,0:T(8,128)(2,1)S(1)} %copy-done.2, f32[1,512]{1,0:T(1,128)S(1)} %bitcast.7, ...), custom_call_target="tpu_custom_call" | custom-call | tf_op jit(solution)/shard_map/mixer/pallas_call | solution.py:155
  18.6 0.0 copy-start
  18.6 0.7 copy-done
  19.3 0.0 copy-done.10
  19.3 1.1 copy.23.router
  20.4 95.1 %mixture.1 = bf16[64,2048]{1,0:T(8,128)(2,1)} custom-call(bf16[512,256]{1,0:T(8,128)(2,1)} %copy-done, bf16[128,2048]{1,0:T(8,128)(2,1)} %alpha.1, bf16[128,2048]{1,0:T(8,128)(2,1)} %beta.1, bf16[64,2048]{1,0:T(8,128)(2,1)} %skip.1, f32[1,2048]{1,0:T(1,128)} %bitcast.10, f32[1,2048]{1,0:T(1,128)} %bitcast.11, f32[1,2048]{1,0:T(1,128)} %bitcast.12, ...), custom_call_target="tpu_custom_call" | custom-call | tf_op jit(solution)/shard_map/mixture/pallas_call | solution.py:529
  115.5 1.7 %copy.25 = bf16[64,2048]{1,0:T(8,128)(2,1)} copy(bf16[64,2048]{1,0:T(8,128)(2,1)} %mixture.1) | data formatting | bytes 524288
  (3 shorter events, 0.0 us)
Async XLA Ops:
  0.0 19.3 %copy-start.10 = (bf16[2048,2]{0,1:T(2,128)(2,1)S(1)}, bf16[2048,2]{0,1:T(2,128)(2,1)}, u32[]{:S(2)}) copy-start(bf16[2048,2]{0,1:T(2,128)(2,1)} %param.37) | copy-start | bytes 24580
  0.9 1.0 copy-start.1
  1.9 1.0 copy-start.2
  2.9 0.9 copy-start.3
  3.9 0.9 copy-start.4
  4.8 0.9 copy-start.5
  5.8 0.9 copy-start.6
  6.8 0.7 copy-start.7
  7.4 0.7 copy-start.8
  8.1 0.7 copy-start.9
  18.6 0.7 copy-start

commit v3 on v2

--- a/solution.py
+++ b/solution.py
@@ -8,6 +8,7 @@
 from jax.sharding import PartitionSpec as P
 
 FF = 2048
+CHUNKS = 4
 EPSILON = 1e-06
 
 
@@ -183,7 +184,7 @@
     ).wait_recv()
 
 
-def line_reduce(z, core, nz, rows, part, twin, box_r, box_l, out_r, out_l, sems, to_right, to_left):
+def line_reduce(z, core, nz, rows, part, twin, box_r, box_l, out_r, out_l, sems, to_right, to_left, eager):
     twin_recv, send_r, recv_r, send_l, recv_l = sems
     chunks = part.shape[1]
     own = pl.ds(pl.multiple_of(core * rows, rows), rows)
@@ -215,18 +216,55 @@
 
             hop(out, box, send, recv, d, ch, to).start()
 
-    def step(tau, _):
+    def right(d):
+        side(d, z > 0, out_r, box_r, send_r, recv_r, to_right)
+
+    def left(d):
+        side(d, z < nz - 1, out_l, box_l, send_l, recv_l, to_left)
+
+    def far_first(tau, _):
         @pl.when((tau >= z) & (z < nz - 1))
         def _():
-            side(nz - 1 + z - tau, z > 0, out_r, box_r, send_r, recv_r, to_right)
+            right(nz - 1 + z - tau)
 
         @pl.when((tau + z >= nz - 1) & (z > 0))
         def _():
-            side(tau + z - (nz - 1), z < nz - 1, out_l, box_l, send_l, recv_l, to_left)
+            left(tau + z - (nz - 1))
 
         return 0
 
-    lax.fori_loop(0, nz - 1, step, 0)
+    def near_first(k, _):
+        d = nz - 1 - k
+        lefts = (d < z) & (z < nz - 1)
+
+        @pl.when(lefts & (z >= nz // 2))
+        def _():
+            left(d)
+
+        @pl.when((k > z) & (z > 0))
+        def _():
+            right(k)
+
+        @pl.when(lefts & (z < nz // 2))
+        def _():
+            left(d)
+
+        return 0
+
+    def run():
+        if eager:
+            lax.fori_loop(1, nz, near_first, 0)
+        else:
+            lax.fori_loop(0, nz - 1, far_first, 0)
+
+    def edge(d):
+        @pl.when((z == 0) & (d > 0))
+        def _():
+            right(d)
+
+        @pl.when((z == nz - 1) & (d < nz - 1))
+        def _():
+            left(d)
 
     def finish(total):
         twin_wait(z)
@@ -258,11 +296,11 @@
 
         lax.fori_loop(0, nz, one, 0)
 
-    return finish, drain
+    return run, edge, finish, drain
 
 
 def experts_kernel(
-    dv, n_sp, nz, cap, pad,
+    dv, n_sp, nz, cap, fold, pad,
     heads, alpha, beta, skip, gain1, gain2, gain3, router, w1, w2, w3, cluster,
     out,
     wcat, w1v, w2v, w3v, part, twin, box_r, box_l, out_r, out_l, mixed, hmid, placing,
@@ -332,10 +370,11 @@
         return 0
 
     lax.fori_loop(0, nz, project, 0)
-    finish, drain = line_reduce(
+    run, _, finish, drain = line_reduce(
         z, core, nz, rows, part, twin, box_r, box_l, out_r, out_l,
-        (tw_r, rs_sr, rs_rr, rs_sl, rs_rl), to_right, to_left,
-    )
+        (tw_r, rs_sr, rs_rr, rs_sl, rs_rl), to_right, to_left, False,
+    )
+    run()
     finish(mixed)
 
     def whole(ref):
@@ -356,16 +395,18 @@
     ).astype(bf)
     counts = jnp.dot(ones.astype(bf), upto, preferred_element_type=f32)
     rank = jnp.sum(ones * counts, axis=0, keepdims=True).astype(jnp.int32) - 1
-    slot = group * pad + rank
-    placing[...] = jnp.where(
-        lax.broadcasted_iota(jnp.int32, (slots, rows), 0) == slot, 1.0, 0.0
-    ).astype(bf)
-    col = lax.broadcasted_iota(jnp.int32, (compact, slots), 1)
-    inner = col & (pad - 1)
-    target = (col >> (pad.bit_length() - 1)) * cap + inner
-    packing = jnp.where(
-        (lax.broadcasted_iota(jnp.int32, (compact, slots), 0) == target) & (inner < cap), 1.0, 0.0
-    ).astype(bf)
+    slot = group * pad + rank * fold
+    slot_id = lax.broadcasted_iota(jnp.int32, (slots, rows), 0)
+    for q in range(fold):
+        placing[q] = jnp.where(slot_id == slot + q, 1.0, 0.0).astype(bf)
+    line_id = lax.broadcasted_iota(jnp.int32, (compact, 1), 0)
+    source = jnp.zeros((compact, 1), jnp.int32)
+    for j in range(1, n_sp):
+        source = source + jnp.where(line_id >= j * cap, 1, 0)
+    first = source * pad + (line_id - source * cap) * fold
+    first = jnp.where(line_id < n_sp * cap, first, -fold)
+    column = lax.broadcasted_iota(jnp.int32, (compact, slots), 1)
+    packing = [jnp.where(column == first + q, 1.0, 0.0).astype(bf) for q in range(fold)]
 
     def sp_copy(src, dst, k, send, recv):
         g = lax.rem(place + k, n_sp)
@@ -382,15 +423,24 @@
             g = lax.rem(place + k, n_sp)
             landed(dst.at[g], recv.at[g], peer)
 
-    sp_out[...] = (
-        jnp.dot(placing[...], normed, preferred_element_type=f32)
-        .astype(bf)
-        .reshape(n_sp, pad, width)
-    )
+    piece = width // fold
+
+    def cut(x, q):
+        return x[:, q * piece : (q + 1) * piece]
+
+    placed = 0.0
+    for q in range(fold):
+        placed = placed + jnp.dot(placing[q], cut(normed, q), preferred_element_type=f32)
+    sp_out[...] = placed.astype(bf).reshape(n_sp, pad, piece)
     sp_exchange(sp_out, sp_in, sp_s, sp_r)
-    packed = jnp.dot(
-        packing, sp_in[...].reshape(slots, width), preferred_element_type=f32
-    ).astype(bf)
+    arrived = sp_in[...].reshape(slots, piece)
+    packed = jnp.concatenate(
+        [
+            jnp.dot(packing[q], arrived, preferred_element_type=f32).astype(bf)
+            for q in range(fold)
+        ],
+        axis=1,
+    )
     mine = pl.ds(pl.multiple_of(core * compact, compact), compact)
     theirs = pl.ds(pl.multiple_of((1 - core) * compact, compact), compact)
     for ch in range(chunks):
@@ -429,6 +479,11 @@
             part2[d, ch] = (weight * y).astype(bf)
         twin_copy(part2, twin2, d, compact, tw2_s, tw2_r).start()
 
+    run2, edge2, finish2, drain2 = line_reduce(
+        z, core, nz, compact, part2, twin2, box_r2, box_l2, out_r2, out_l2,
+        (tw2_r, rs2_sr, rs2_rr, rs2_sl, rs2_rl), to_right, to_left, True,
+    )
+
     def gather(tau, _):
         low, high = z - tau, z + tau
         for ch in range(chunks):
@@ -461,27 +516,33 @@
         @pl.when(low >= 0)
         def _():
             expert(low)
+            edge2(low)
 
         @pl.when((high < nz) & (tau > 0))
         def _():
             expert(high)
+            edge2(high)
 
         return 0
 
     lax.fori_loop(0, nz, gather, 0)
-    finish2, drain2 = line_reduce(
-        z, core, nz, compact, part2, twin2, box_r2, box_l2, out_r2, out_l2,
-        (tw2_r, rs2_sr, rs2_rr, rs2_sl, rs2_rl), to_right, to_left,
-    )
+    run2()
     finish2(summed)
-    back_out[...] = (
-        lax.dot_general(packing, whole(summed).astype(bf), TN, preferred_element_type=f32)
-        .astype(bf)
-        .reshape(n_sp, pad, width)
-    )
+    total = whole(summed).astype(bf)
+    placed = 0.0
+    for q in range(fold):
+        placed = placed + lax.dot_general(
+            packing[q], cut(total, q), TN, preferred_element_type=f32
+        )
+    back_out[...] = placed.astype(bf).reshape(n_sp, pad, piece)
     sp_exchange(back_out, back_in, bk_s, bk_r)
-    routed = lax.dot_general(
-        placing[...], back_in[...].reshape(slots, width), TN, preferred_element_type=f32
+    arrived = back_in[...].reshape(slots, piece)
+    routed = jnp.concatenate(
+        [
+            lax.dot_general(placing[q], arrived, TN, preferred_element_type=f32)
+            for q in range(fold)
+        ],
+        axis=1,
     )
     out[...] = (hmid[...].astype(f32) + rms_scale(routed, gain3[...])).astype(bf)
 
@@ -514,11 +575,11 @@
     n_sp, nz = lax.axis_size("sp"), lax.axis_size("tp") // 2
     rows, width = skip.shape
     cap = (9 * rows + 8 * n_sp - 1) // (8 * n_sp)
-    pad = 16
-    while pad < cap:
-        pad *= 2
+    fold = 4
+    pad = (cap * fold + 15) // 16 * 16
     compact = (n_sp * cap + 15) // 16 * 16
-    chunks, half = 2, width // 2
+    chunks = CHUNKS
+    half = width // chunks
     f32, bf = jnp.float32, jnp.bfloat16
     vm = pl.BlockSpec(memory_space=pltpu.VMEM)
     hbm = pl.BlockSpec(memory_space=pl.ANY)
@@ -527,7 +588,7 @@
     dma = pltpu.SemaphoreType.DMA
     reduce_sems = [dma((nz,))] * 2 + [dma((nz, chunks))] * 4
     return pl.pallas_call(
-        functools.partial(experts_kernel, dv, n_sp, nz, cap, pad),
+        functools.partial(experts_kernel, dv, n_sp, nz, cap, fold, pad),
         out_shape=jax.ShapeDtypeStruct(skip.shape, bf),
         in_specs=[vm] * 8 + [hbm] * 3 + [vm],
         out_specs=vm,
@@ -542,17 +603,17 @@
         + [
             pltpu.VMEM(line[1:], f32),
             pltpu.VMEM(skip.shape, bf),
-            pltpu.VMEM((n_sp * pad, rows), bf),
-            pltpu.VMEM((n_sp, pad, width), bf),
-            pltpu.VMEM((n_sp, pad, width), bf),
+            pltpu.VMEM((fold, n_sp * pad, rows), bf),
+            pltpu.VMEM((n_sp, pad, width // fold), bf),
+            pltpu.VMEM((n_sp, pad, width // fold), bf),
             pltpu.VMEM((nz, chunks, 2 * compact, half), bf),
             pltpu.VMEM((nz, chunks, 2 * compact, half), bf),
         ]
         + [pltpu.VMEM(line2, bf)] * 5
         + [
             pltpu.VMEM(line2[1:], f32),
-            pltpu.VMEM((n_sp, pad, width), bf),
-            pltpu.VMEM((n_sp, pad, width), bf),
+            pltpu.VMEM((n_sp, pad, width // fold), bf),
+            pltpu.VMEM((n_sp, pad, width // fold), bf),
             dma((3,)),
         ]
         + reduce_sems

time: 118 us -> 110 us (0.932)
  Pallas kernels: 105 us -> 97.4 us
    pallas_call x1, Pallas kernels: 95.1 us -> 87.5 us  [mixture(): pl.pallas_call(functools.partial(experts_kernel, dv, n_sp, nz, cap, fold,...]
where the time goes in v3:
time: 110 us
  Pallas kernels  97.4 us (89%)
  local copies, waits for them, and re-layouts  12.2 us (11%)
    pallas_call x1, Pallas kernels, mixture(): pl.pallas_call(functools.partial(experts_kernel, dv, n_sp, nz, cap, fold,...  87.5 us
    unnamed x25, local copies, waits for them, and re-layouts  12.2 us
    pallas_call x1, Pallas kernels, mixer(): pl.pallas_call(functools.partial(mixer_kernel, n_sp, heads, ka, kb, dv),...  9.83 us

profile of v3, /device:TPU:0, one launch (start us, length us, event | category | flops | bytes accessed | tf_op | source)
XLA Modules:
  0.0 109.6 jit_solution(5347877821148434016)
XLA Ops:
  0.0 0.0 copy-start.10
  0.0 0.8 copy.22.bias
  0.9 0.0 copy-start.1
  0.9 1.0 copy-done.1
  1.9 0.0 copy-start.2
  1.9 1.0 copy-done.2
  2.9 0.0 copy-start.3
  3.0 0.9 copy-done.3
  3.9 0.0 copy-start.4
  3.9 0.9 copy-done.4
  4.8 0.0 copy-start.5
  4.9 0.9 copy-done.5
  5.8 0.0 copy-start.6
  5.8 0.9 copy-done.6
  6.8 0.7 copy-done.7
  7.4 0.7 copy-done.8
  8.1 0.7 copy-done.9
  8.8 9.8 %mixer.1.heads = bf16[512,256]{1,0:T(8,128)(2,1)S(1)} custom-call(bf16[512,256]{1,0:T(8,128)(2,1)S(1)} %copy-done.3, bf16[512,256]{1,0:T(8,128)(2,1)S(1)} %copy-done.4, f32[1,256]{1,0:T(1,128)S(1)} %bitcast.8, bf16[512,512]{1,0:T(8,128)(2,1)S(1)} %copy-done.1, bf16[512,512]{1,0:T(8,128)(2,1)S(1)} %copy-done.2, f32[1,512]{1,0:T(1,128)S(1)} %bitcast.7, ...), custom_call_target="tpu_custom_call" | custom-call | tf_op jit(solution)/shard_map/mixer/pallas_call | solution.py:156
  18.6 0.0 copy-start
  18.6 0.7 copy-done
  19.3 0.0 copy-done.10
  19.3 1.1 copy.23.router
  20.4 87.5 %mixture.1 = bf16[64,2048]{1,0:T(8,128)(2,1)} custom-call(bf16[512,256]{1,0:T(8,128)(2,1)} %copy-done, bf16[128,2048]{1,0:T(8,128)(2,1)} %alpha.1, bf16[128,2048]{1,0:T(8,128)(2,1)} %beta.1, bf16[64,2048]{1,0:T(8,128)(2,1)} %skip.1, f32[1,2048]{1,0:T(1,128)} %bitcast.10, f32[1,2048]{1,0:T(1,128)} %bitcast.11, f32[1,2048]{1,0:T(1,128)} %bitcast.12, ...), custom_call_target="tpu_custom_call" | custom-call | tf_op jit(solution)/shard_map/mixture/pallas_call | solution.py:590
  107.9 1.7 %copy.25 = bf16[64,2048]{1,0:T(8,128)(2,1)} copy(bf16[64,2048]{1,0:T(8,128)(2,1)} %mixture.1) | data formatting | bytes 524288
  (3 shorter events, 0.0 us)
Async XLA Ops:
  0.0 19.3 %copy-start.10 = (bf16[2048,2]{0,1:T(2,128)(2,1)S(1)}, bf16[2048,2]{0,1:T(2,128)(2,1)}, u32[]{:S(2)}) copy-start(bf16[2048,2]{0,1:T(2,128)(2,1)} %param.37) | copy-start | bytes 24580
  0.9 1.0 copy-start.1
  1.9 1.0 copy-start.2
  2.9 0.9 copy-start.3
  3.9 0.9 copy-start.4
  4.8 0.9 copy-start.5
  5.8 0.9 copy-start.6
  6.8 0.7 copy-start.7
  7.4 0.7 copy-start.8
  8.1 0.7 copy-start.9
  18.6 0.7 copy-start
